TPU v7x, 32 devices: a whole 2x2x4 slice. The times are simulated.
32 devices in a mesh: sp: 8 (over z, x), tp: 4 (over y, core).
Axes of the slice: x: 2, y: 2, z: 4, core: 2. Of those that a mesh axis runs over, the one named last changes fastest.
Arguments:
- latent: bfloat16 [4096, 4096], P('sp'), may hold values from -64 to 64
- context: bfloat16 [512, 4096], P('sp'), may hold values from -6 to 6
- condition: bfloat16 [4096], P('sp'), may hold values from -6 to 6
- context_condition: bfloat16 [4096], P('sp'), may hold values from -6 to 6
- shift_weight: bfloat16 [4096, 4096], P('sp', 'tp'), may hold values from -0.125 to 0.125
- scale_weight: bfloat16 [4096, 4096], P('sp', 'tp'), may hold values from -0.125 to 0.125
- gate_weight: bfloat16 [4096, 4096], P('sp', 'tp'), may hold values from -0.25 to 0.25
- norm_gain: float32 [4096], replicated, may hold values from 0.1 to 1.9
- query_weight: bfloat16 [4096, 2048], P(None, 'tp'), may hold values from -0.09375 to 0.09375
- key_weight: bfloat16 [4096, 2048], P(None, 'tp'), may hold values from -0.09375 to 0.09375
- value_weight: bfloat16 [4096, 2048], P(None, 'tp'), may hold values from -0.09375 to 0.09375
- write_weight: bfloat16 [4096, 2, 16], replicated, may hold values from -0.09375 to 0.09375
- decay_weight: bfloat16 [4096, 2, 16], replicated, may hold values from -0.09375 to 0.09375
- write_bias: float32 [2, 16], replicated, may hold values from -12 to 1
- decay_bias: float32 [2, 16], replicated, may hold values from -16 to -4
- log_rate: float32 [2, 16], replicated, may hold values from 0 to 1.4
- head_gain: float32 [128], replicated, may hold values from 0.1 to 1.9
- out_weight: bfloat16 [2048, 4096], P(None, 'tp'), may hold values from -0.125 to 0.125
Outputs:
- updated: bfloat16 [4096, 4096], P('sp', 'tp')
All inputs are finite; a program needn't handle non-finite values.
Results may differ from a plain program's by a relative error of at most 0.013.
Values may be sent and summed in bfloat16 or wider, within the bound.
A program may use at most 128 MiB of HBM per device.

v0:
```python
import jax
import jax.numpy as jnp
from jax import lax
from jax.sharding import PartitionSpec as P

HEAD_DIM = 128
BLOCK = 64


epsilon = 0.0001
highest = lax.Precision.HIGHEST


def prefix(shard, axis, combine, identity, reverse):
    peers, place = (lax.axis_size(axis), lax.axis_index(axis))
    everything = jax.tree.map(
        lambda part, kind: lax.all_gather(part.astype(kind), axis),
        shard,
        (jnp.bfloat16, jnp.bfloat16),
    )
    start = jax.tree.map(
        lambda part, zero: jnp.broadcast_to(jnp.asarray(zero, part.dtype), part.shape),
        shard,
        identity,
    )

    def lap(k, before):
        at = peers - 1 - k if reverse else k
        reached = at > place if reverse else at < place
        new = combine(
            before, jax.tree.map(lambda part, own: part[at].astype(own.dtype), everything, shard)
        )
        return jax.tree.map(lambda a, b: jnp.where(reached, a, b), new, before)

    return lax.fori_loop(0, peers, lap, start)


def rms_rows(row_data, row_gain):
    values = row_data.astype(jnp.float32)
    scaled = values * lax.rsqrt(jnp.mean(values * values, axis=-1, keepdims=True) + epsilon)
    return scaled * row_gain


def unit_heads(matrix, head_count):
    split_heads = matrix.astype(jnp.float32).reshape(matrix.shape[0], head_count, -1)
    return split_heads * lax.rsqrt(
        jnp.sum(split_heads * split_heads, axis=-1, keepdims=True) + epsilon
    )


def head_gates(write_pre, decay_pre, write_bias, decay_bias, log_rate):
    write_rate = jax.nn.sigmoid(write_pre.astype(jnp.float32) + write_bias)
    log_decay = -jnp.exp(log_rate) * jax.nn.softplus(decay_pre.astype(jnp.float32) + decay_bias)
    return (write_rate, log_decay)


def project(matrix, weight):
    return jnp.dot(matrix, weight, preferred_element_type=jnp.float32).astype(jnp.bfloat16)


def to_blocks(source, span):
    heads_first = jnp.moveaxis(source, 1, 0)
    block_count = heads_first.shape[1] // span
    return heads_first.reshape((heads_first.shape[0], block_count, span) + heads_first.shape[2:])


def prepare_keys(key_vecs, value_vecs, log_decay, write_rate):
    span = min(BLOCK, key_vecs.shape[0])
    block_keys = to_blocks(key_vecs, span)
    block_values = to_blocks(value_vecs, span)
    running = jnp.cumsum(to_blocks(log_decay, span), axis=-1)
    block_rates = to_blocks(write_rate, span)
    offsets = jnp.arange(span)
    lower_mask = offsets[:, None] >= offsets[None, :]
    strict_mask = offsets[:, None] > offsets[None, :]
    spread = running[..., :, None] - running[..., None, :]
    decay_mat = jnp.where(lower_mask, jnp.exp(jnp.where(lower_mask, spread, 0.0)), 0.0)
    scaled = block_keys * block_rates[..., None]
    system = jnp.einsum("hnid,hnjd->hnij", scaled, block_keys, precision=highest) * decay_mat
    system = jnp.where(strict_mask, system, 0.0) + jnp.eye(span, dtype=system.dtype)
    value_width = block_values.shape[-1]
    both_sides = jnp.concatenate(
        [block_values * block_rates[..., None], scaled * jnp.exp(running)[..., None]], axis=-1
    )
    solved = jax.scipy.linalg.solve_triangular(system, both_sides, lower=True, unit_diagonal=True)
    fresh_values = solved[..., :value_width]
    key_weights = solved[..., value_width:]
    last_gate = running[..., -1]
    late_keys = block_keys * jnp.exp(last_gate[..., None] - running)[..., None]
    return (block_keys, running, decay_mat, fresh_values, key_weights, last_gate, late_keys)


def prepare_queries(query_vecs, prepared):
    block_queries = to_blocks(query_vecs, prepared[0].shape[2])
    query_keys = (
        jnp.einsum("hnid,hnjd->hnij", block_queries, prepared[0], precision=highest) * prepared[2]
    )
    early_queries = block_queries * jnp.exp(prepared[1])[..., None]
    return (query_keys, early_queries)


def run_blocks(prepared, queried, start):
    inputs = tuple(
        (
            jnp.moveaxis(item, 1, 0)
            for item in (prepared[3], prepared[4], queried[0], queried[1], prepared[6], prepared[5])
        )
    )

    def advance(carried, pieces):
        new_in, key_in, score_in, query_in, late_in, gate_in = pieces
        corrected = new_in - jnp.einsum("hcd,hde->hce", key_in, carried, precision=highest)
        output = jnp.einsum("hcd,hde->hce", query_in, carried, precision=highest)
        output = output + jnp.einsum("hij,hje->hie", score_in, corrected, precision=highest)
        carried = carried * jnp.exp(gate_in)[:, None, None] + jnp.einsum(
            "hcd,hce->hde", late_in, corrected, precision=highest
        )
        return (carried, output)

    closing, outputs = lax.scan(advance, start, inputs)
    merged = jnp.transpose(outputs, (0, 2, 1, 3))
    return merged.reshape(-1, merged.shape[2], merged.shape[3])


def block_maps(prepared):
    late_keys = prepared[6]
    head_count = late_keys.shape[0]
    width = late_keys.shape[-1]
    identity = jnp.broadcast_to(jnp.eye(width, dtype=jnp.float32), (head_count, width, width))
    zero_offset = jnp.zeros((head_count, width, prepared[3].shape[-1]), jnp.float32)
    inputs = tuple(
        (jnp.moveaxis(item, 1, 0) for item in (prepared[6], prepared[4], prepared[3], prepared[5]))
    )

    def block_absorb(map_pair, pieces):
        transfer, offset = map_pair
        late_in, key_in, new_in, gate_in = pieces
        step_map = identity * jnp.exp(gate_in)[:, None, None] - jnp.einsum(
            "hcd,hce->hde", late_in, key_in, precision=highest
        )
        transfer = jnp.einsum("hij,hjk->hik", step_map, transfer, precision=highest)
        offset = jnp.einsum("hij,hjk->hik", step_map, offset, precision=highest) + jnp.einsum(
            "hcd,hce->hde", late_in, new_in, precision=highest
        )
        return ((transfer, offset), None)

    result_pair, unused = lax.scan(block_absorb, (identity, zero_offset), inputs)
    return result_pair


def compose(first_map, second_map):
    transfer = jnp.einsum("hij,hjk->hik", second_map[0], first_map[0], precision=highest)
    offset = (
        jnp.einsum("hij,hjk->hik", second_map[0], first_map[1], precision=highest) + second_map[1]
    )
    return (transfer, offset)


def apply_map(map_pair, start):
    return jnp.einsum("hij,hjk->hik", map_pair[0], start, precision=highest) + map_pair[1]


def chain_offset(transfers, offsets, backwards):
    identity = jnp.broadcast_to(jnp.eye(transfers.shape[2], dtype=jnp.float32), transfers.shape[1:])
    zero_offset = jnp.zeros(offsets.shape[1:], jnp.float32)

    def chain_absorb(running_map, next_map):
        return (compose(running_map, next_map), None)

    total, unused = lax.scan(
        chain_absorb, (identity, zero_offset), (transfers, offsets), reverse=backwards
    )
    return total[1]


def body(
    latent,
    context,
    condition,
    context_condition,
    shift_weight,
    scale_weight,
    gate_weight,
    norm_gain,
    query_weight,
    key_weight,
    value_weight,
    write_weight,
    decay_weight,
    write_bias,
    decay_bias,
    log_rate,
    head_gain,
    out_weight,
):
    heads_here = query_weight.shape[1] // HEAD_DIM
    first_head = lax.axis_index("tp") * heads_here
    own_cols = gate_weight.shape[1]
    col_start = lax.axis_index("tp") * own_cols
    stacked = jnp.stack([condition, context_condition]).astype(jnp.float32)
    silu_rows = jax.nn.silu(stacked).astype(jnp.bfloat16)
    part_shift = jnp.dot(silu_rows, shift_weight, preferred_element_type=jnp.float32)
    part_scale = jnp.dot(silu_rows, scale_weight, preferred_element_type=jnp.float32)
    part_gate = jnp.dot(silu_rows[:1], gate_weight, preferred_element_type=jnp.float32)
    shift_part, scale_part, gate_row = lax.psum((part_shift, part_scale, part_gate), "sp")
    shift_rows, scale_rows = (
        lax.all_gather(shift_part, "tp", axis=1, tiled=True),
        lax.all_gather(scale_part, "tp", axis=1, tiled=True),
    )

    def modulate(row_data, row_index):
        normed = rms_rows(row_data, norm_gain)
        return (normed * (1.0 + scale_rows[row_index]) + shift_rows[row_index]).astype(jnp.bfloat16)

    write_here = lax.dynamic_slice_in_dim(write_weight, first_head, heads_here, 2).reshape(
        write_weight.shape[0], -1
    )
    decay_here = lax.dynamic_slice_in_dim(decay_weight, first_head, heads_here, 2).reshape(
        decay_weight.shape[0], -1
    )
    bias_write = lax.dynamic_slice_in_dim(write_bias, first_head, heads_here, 1)
    bias_decay = lax.dynamic_slice_in_dim(decay_bias, first_head, heads_here, 1)
    rate_here = lax.dynamic_slice_in_dim(log_rate, first_head, heads_here, 1)

    def key_inputs(modulated):
        return (
            project(modulated, key_weight),
            project(modulated, value_weight),
            project(modulated, write_here).reshape(-1, 2, heads_here),
            project(modulated, decay_here).reshape(-1, 2, heads_here),
        )

    ctx_key, ctx_value, ctx_write, ctx_decay = key_inputs(modulate(context, 1))
    ctx_keys = unit_heads(ctx_key, heads_here)
    ctx_values = ctx_value.astype(jnp.float32).reshape(-1, heads_here, HEAD_DIM)
    ctx_rate, ctx_log = head_gates(ctx_write, ctx_decay, bias_write, bias_decay, rate_here)
    ctx_fwd_transfer, ctx_fwd_offset = block_maps(
        prepare_keys(ctx_keys, ctx_values, ctx_log[:, 0], ctx_rate[:, 0])
    )
    ctx_bwd_transfer, ctx_bwd_offset = block_maps(
        prepare_keys(
            jnp.flip(ctx_keys, 0),
            jnp.flip(ctx_values, 0),
            jnp.flip(ctx_log[:, 1], 0),
            jnp.flip(ctx_rate[:, 1], 0),
        )
    )
    all_maps = (
        lax.all_gather(
            ctx_fwd_transfer[None].astype(jnp.bfloat16), "sp", axis=0, tiled=True
        ).astype(jnp.float32),
        lax.all_gather(ctx_fwd_offset[None].astype(jnp.bfloat16), "sp", axis=0, tiled=True).astype(
            jnp.float32
        ),
        lax.all_gather(
            ctx_bwd_transfer[None].astype(jnp.bfloat16), "sp", axis=0, tiled=True
        ).astype(jnp.float32),
        lax.all_gather(ctx_bwd_offset[None].astype(jnp.bfloat16), "sp", axis=0, tiled=True).astype(
            jnp.float32
        ),
    )
    ctx_forward = chain_offset(all_maps[0], all_maps[1], False)
    ctx_backward = chain_offset(all_maps[2], all_maps[3], True)
    modulated = modulate(latent, 0)
    queries = unit_heads(project(modulated, query_weight), heads_here) * HEAD_DIM ** (-0.5)
    lat_key, lat_value, lat_write, lat_decay = key_inputs(modulated)
    key_vecs = unit_heads(lat_key, heads_here)
    value_vecs = lat_value.astype(jnp.float32).reshape(-1, heads_here, HEAD_DIM)
    write_rate, log_decay = head_gates(lat_write, lat_decay, bias_write, bias_decay, rate_here)
    forward_prep = prepare_keys(key_vecs, value_vecs, log_decay[:, 0], write_rate[:, 0])
    backward_prep = prepare_keys(
        jnp.flip(key_vecs, 0),
        jnp.flip(value_vecs, 0),
        jnp.flip(log_decay[:, 1], 0),
        jnp.flip(write_rate[:, 1], 0),
    )
    fwd_transfer, fwd_offset = block_maps(forward_prep)
    bwd_transfer, bwd_offset = block_maps(backward_prep)
    identity = jnp.broadcast_to(jnp.eye(HEAD_DIM, dtype=jnp.float32), fwd_transfer.shape)
    zero_offset = jnp.zeros_like(fwd_offset)
    before_forward = prefix(
        (fwd_transfer, fwd_offset), "sp", compose, (identity, zero_offset), False
    )
    before_backward = prefix(
        (bwd_transfer, bwd_offset), "sp", compose, (identity, zero_offset), True
    )
    start_forward = apply_map(before_forward, ctx_forward)
    start_backward = apply_map(before_backward, ctx_backward)
    forward_out = run_blocks(forward_prep, prepare_queries(queries, forward_prep), start_forward)
    backward_out = jnp.flip(
        run_blocks(
            backward_prep, prepare_queries(jnp.flip(queries, 0), backward_prep), start_backward
        ),
        0,
    )
    combined = forward_out + backward_out
    head_out = (
        combined
        * lax.rsqrt(jnp.mean(combined * combined, axis=-1, keepdims=True) + epsilon)
        * head_gain
    )
    head_out = head_out.astype(jnp.bfloat16).reshape(combined.shape[0], -1)
    branch = jnp.dot(
        lax.all_gather(head_out, "tp", axis=1, tiled=True),
        out_weight,
        preferred_element_type=jnp.float32,
    )
    residual = lax.dynamic_slice_in_dim(latent, col_start, own_cols, 1).astype(jnp.float32)
    return (residual + gate_row * branch).astype(jnp.bfloat16)


def solution(mesh):
    placed = (
        P("sp", None),
        P("sp", None),
        P("sp"),
        P("sp"),
        P("sp", "tp"),
        P("sp", "tp"),
        P("sp", "tp"),
        P(),
        P(None, "tp"),
        P(None, "tp"),
        P(None, "tp"),
        P(),
        P(),
        P(),
        P(),
        P(),
        P(),
        P(None, "tp"),
    )
    return jax.shard_map(body, mesh=mesh, in_specs=placed, out_specs=P("sp", "tp"), check_vma=False)
```

profile of v0, /device:TPU:0, one launch (start us, length us, event | category | flops | bytes accessed | tf_op | source)
XLA Modules:
  0.0 847.8 jit_solution(8422215382030809919)
XLA Ops:
  11.3 39.4 %all-reduce = (f32[2,1024]{1,0:T(2,128)S(1)}, f32[2,1024]{1,0:T(2,128)S(1)}, f32[1024]{0:T(1024)}) all-reduce(f32[2,1024]{1,0:T(2,128)S(1)} %fusion.255, f32[2,1024]{1,0:T(2,128)S(1)} %fusion.254, f32[1024]{0:T(1024)S(1)} %bitcast.539), channel_id=1, replica_groups=mesh['sp'=8,'tp'=4] {'sp'}, use_global_device_ids=true, to_apply=%region_3.4 | all-reduce | flops 5120 | bytes 40960 | tf_op jit(solution)/shard_map/psum | solution.py:205
  50.8 5.2 all_gather.45
  56.5 5.2 all_gather.46
  62.3 3.1 fusion.108
  66.5 4.1 fusion.112
  76.4 3.4 fusion.179
  80.6 5.9 fusion.186
  88.1 5.9 multiply_reduce_fusion.1
  95.1 5.8 convolution_convert_fusion.1
  104.6 158.0 %custom-call.14 = f32[4,8,1,64,64]{3,4,2,1,0:T(8,128)} custom-call(f32[4,8,1,64,64]{4,3,2,1,0:T(8,128)S(1)} %fusion.160), custom_call_target="InvertDiagBlocksLowerTriangular" | custom-call | tf_op jit(solution)/shard_map/jit(_solve_triangular)/vmap(vmap())/triangular_solve | solution.py:85
  265.1 3.0 multiply_multiply_fusion.1
  274.4 37.6 %while.122 = (s32[]{:T(128)}, f32[4,128,128]{2,1,0:T(8,128)S(1)}, f32[4,128,128]{2,1,0:T(8,128)S(1)}, f32[8,4]{1,0:T(8,128)}, f32[8,4,64,128]{3,2,1,0:T(8,128)},...) while((s32[]{:T(128)}, f32[4,128,128]{2,1,0:T(8,128)S(1)}, ...), condition=%wide.region_7.9_spmd.clone, body=%wide.region_6.8_spmd.clone.sunk | while | flops 302252032 | bytes 3475619 | solution.py:147
  316.3 3.2 fusion.173
  321.2 3.1 fusion.172
  325.0 19.7 %custom-call.15 = f32[4,1,64,64]{2,3,1,0:T(8,128)S(1)} custom-call(f32[4,1,64,64]{3,2,1,0:T(8,128)S(1)} %fusion.176), custom_call_target="InvertDiagBlocksLowerTriangular" | custom-call | tf_op jit(solution)/shard_map/jit(_solve_triangular)/vmap()/triangular_solve | solution.py:85
  355.4 20.4 %custom-call.17 = f32[4,1,64,64]{2,3,1,0:T(8,128)S(1)} custom-call(f32[4,1,64,64]{3,2,1,0:T(8,128)} %fusion.178), custom_call_target="InvertDiagBlocksLowerTriangular" | custom-call | tf_op jit(solution)/shard_map/jit(_solve_triangular)/vmap()/triangular_solve | solution.py:85
  382.9 8.8 %rev.37 = f32[512,4,128]{0,2,1:T(8,128)} reverse(bf16[512,4,128]{0,2,1:T(8,128)(2,1)} %bitcast.507), dimensions={0} | reverse | bytes 1572864 | tf_op jit(solution)/shard_map/jit(_flip)/rev | solution.py:273
  396.1 5.9 rev.35
  403.5 8.9 %reverse.3 = f32[512,4,128]{2,0,1:T(8,128)} reverse(f32[512,4,128]{2,0,1:T(8,128)} %get-tuple-element.1036), dimensions={0} | reverse | bytes 2097152 | tf_op jit(solution)/shard_map/reverse
  417.3 3.8 fusion.145
  421.1 158.7 %custom-call.16 = f32[4,8,1,64,64]{3,4,2,1,0:T(8,128)} custom-call(f32[4,8,1,64,64]{4,3,2,1,0:T(8,128)} %fusion.145), custom_call_target="InvertDiagBlocksLowerTriangular" | custom-call | tf_op jit(solution)/shard_map/jit(_solve_triangular)/vmap(vmap())/triangular_solve | solution.py:85
  579.8 3.1 multiply_multiply_fusion
  588.4 32.2 %while.125 = (s32[]{:T(128)}, f32[4,128,128]{2,1,0:T(8,128)S(1)}, f32[4,128,128]{2,1,0:T(8,128)S(1)}, f32[8,4]{1,0:T(8,128)S(1)}, f32[8,4,64,128]{3,2,1,0:T(8,12...) while((s32[]{:T(128)}, f32[4,128,128]{2,1,0:T(8,128)S(1)}, ...), condition=%wide.region_20.23_spmd.clone, body=%wide.region_19.22_spmd.clone.sunk | while | flops 302252032 | bytes 3475619 | solution.py:147
  626.8 4.0 fusion.131
  630.8 33.3 %while.123 = (s32[]{:T(128)}, f32[4,128,128]{2,1,0:T(8,128)S(1)}, f32[4,128,128]{2,1,0:T(8,128)}, s32[]{:T(128)}, bf16[8,4,128,128]{3,2,1,0:T(8,128)(2,1)}, /*in...) while((s32[]{:T(128)}, f32[4,128,128]{2,1,0:T(8,128)S(1)}, f32[4,128,128]{2,1,0:T(8,128)}, ...), condition=%wide.region_9.11_spmd.clone, body=%wide.region_8.10_spmd.clone.sunk | while | flops 201719808 | bytes 3017832 | solution.py:35
  669.9 11.8 %while.124 = (s32[]{:T(128)}, f32[4,128,128]{2,1,0:T(8,128)S(1)}, f32[8,4,128,128]{3,2,1,0:T(8,128)}, f32[8,4,128,128]{3,2,1,0:T(8,128)}, s32[]{:T(128)}, /*index=5*/s32[]{:T(128)}) while((s32[]{:T(128)}, f32[4,128,128]{2,1,0:T(8,128)S(1)}, f32[8,4,128,128]{3,2,1,0:T(8,128)}, f32[8,4,128,128]{3,2,1,0:T(8,128)}, s32[]{:T(128)}, ...), condition=%wide.region_14.17_spmd.clone, body=%wide.region_13.16_spmd.clone.sunk | while | flops 100794368 | bytes 1573967 | solution.py:170
  682.3 48.3 %while.120 = (s32[]{:T(128)}, f32[4,128,128]{2,1,0:T(8,128)S(1)}, f32[8,4,64,128]{3,2,0,1:T(8,128)S(1)}, f32[8,4]{1,0:T(8,128)}, f32[8,4,64,128]{3,2,1,0:T(8,128...) while((s32[]{:T(128)}, f32[4,128,128]{2,1,0:T(8,128)S(1)}, ...), condition=%wide.region_17.20_spmd, body=%wide.region_16.19_spmd.sunk | while | flops 176357376 | bytes 2493593 | solution.py:120
  736.3 11.8 %while.127 = (s32[]{:T(128)}, f32[4,128,128]{2,1,0:T(8,128)S(1)}, f32[8,4,128,128]{3,2,1,0:T(8,128)}, f32[8,4,128,128]{3,2,1,0:T(8,128)}, s32[]{:T(128)}, /*index=5*/s32[]{:T(128)}, s32[]{:T(128)}) while((s32[]{:T(128)}, f32[4,128,128]{2,1,0:T(8,128)S(1)}, f32[8,4,128,128]{3,2,1,0:T(8,128)}, f32[8,4,128,128]{3,2,1,0:T(8,128)}, ...), condition=%wide.region_25.28_spmd.clone, body=%wide.region_24.27_spmd.clone.sunk | while | flops 100794368 | bytes 1574498 | solution.py:170
  748.2 20.4 %while.126 = (s32[]{:T(128)}, f32[4,128,128]{2,1,0:T(8,128)S(1)}, f32[4,128,128]{2,1,0:T(8,128)S(1)}, s32[]{:T(128)}, bf16[8,4,128,128]{3,2,1,0:T(8,128)(2,1)}, ...) while((s32[]{:T(128)}, f32[4,128,128]{2,1,0:T(8,128)S(1)}, ...), condition=%wide.region_22.25_spmd.clone, body=%wide.region_21.24_spmd.clone.sunk | while | flops 201719808 | bytes 3017386 | solution.py:35
  769.1 42.9 %while.121 = (s32[]{:T(128)}, f32[4,128,128]{2,1,0:T(8,128)S(1)}, f32[8,4,64,128]{3,2,0,1:T(8,128)S(1)}, f32[8,4]{1,0:T(8,128)S(1)}, f32[8,4,64,128]{3,2,1,0:T(8...) while((s32[]{:T(128)}, f32[4,128,128]{2,1,0:T(8,128)S(1)}, ...), condition=%wide.region_27.30_spmd, body=%wide.region_26.29_spmd.sunk | while | flops 176357376 | bytes 2493593 | solution.py:120
  814.3 20.0 %all-gather.18.cloned.1.call-done = bf16[512,2048]{0,1:T(8,128)(2,1)} async-done(((bf16[512,512]{0,1:T(8,128)(2,1)}), bf16[512,2048]{0,1:T(8,128)(2,1)}) %all-gather.18.cloned.1.call-update) | async-done | bytes 2097168 | tf_op jit(solution)/shard_map/all_gather | solution.py:304
  834.4 6.5 add_convert_fusion
  (519 shorter events, 325.3 us)
Async XLA Ops:
  6.5 60.0 %copy-start.18 = (f32[4096]{0:T(1024)S(1)}, f32[4096]{0:T(1024)}, u32[]{:S(2)}) copy-start(f32[4096]{0:T(1024)} %param.45) | copy-start | bytes 49156
  6.5 624.3 %all-gather.20.cloned.1.call-start = ((), (), s32[]{:S(2)}) async-start(), calls=%async_computation.1 | async-start | bytes 1179648 | tf_op jit(solution)/shard_map/all_gather | solution.py:17
  6.6 96.0 %copy-start.24 = (f32[64,64]{1,0:T(8,128)}, f32[64,64]{1,0:T(8,128)S(1)}, u32[]{:S(2)}) copy-start(f32[64,64]{1,0:T(8,128)S(1)} %get-tuple-element.1087) | copy-start | bytes 49156
  6.6 96.0 %copy-start.37 = (pred[64,64]{1,0:T(8,128)(4,1)}, pred[64,64]{1,0:T(8,128)(4,1)S(1)}, u32[]{:S(2)}) copy-start(pred[64,64]{1,0:T(8,128)(4,1)S(1)} %get-tuple-element.1086) | copy-start | bytes 12292
  6.6 96.0 %copy-start.26 = (f32[64,64]{1,0:T(8,128)}, f32[64,64]{1,0:T(8,128)S(1)}, u32[]{:S(2)}) copy-start(f32[64,64]{1,0:T(8,128)S(1)} %fusion.220) | copy-start | bytes 49156
  74.0 12.5 %copy-start.31 = (f32[2,4]{1,0:T(2,128)}, f32[2,4]{1,0:T(2,128)S(1)}, u32[]{:S(2)}) copy-start(f32[2,4]{1,0:T(2,128)S(1)} %get-tuple-element.1080) | copy-start | bytes 100
  76.4 10.1 %copy-start.17 = (bf16[4096,8]{0,1:T(8,128)(2,1)}, bf16[4096,8]{0,1:T(8,128)(2,1)S(1)}, u32[]{:S(2)}) copy-start(bf16[4096,8]{0,1:T(8,128)(2,1)S(1)} %reshape.349) | copy-start | bytes 196612
  100.9 164.2 %copy-start.11 = (bf16[512,512]{0,1:T(8,128)(2,1)}, bf16[512,512]{0,1:T(8,128)(2,1)S(1)}, u32[]{:S(2)}) copy-start(bf16[512,512]{0,1:T(8,128)(2,1)S(1)} %convolution_convert_fusion.1) | copy-start | bytes 1572868
  102.5 165.6 %copy-start.22 = (pred[64,64]{1,0:T(8,128)(4,1)}, pred[64,64]{1,0:T(8,128)(4,1)S(1)}, u32[]{:S(2)}) copy-start(pred[64,64]{1,0:T(8,128)(4,1)S(1)} %get-tuple-element.1085) | copy-start | bytes 12292
  102.5 165.6 %copy-start.40 = (pred[64,64]{1,0:T(8,128)(4,1)}, pred[64,64]{1,0:T(8,128)(4,1)S(1)}, u32[]{:S(2)}) copy-start(pred[64,64]{1,0:T(8,128)(4,1)S(1)} %get-tuple-element.1084) | copy-start | bytes 12292
  274.4 39.2 %copy-start.9 = (bf16[64,4096]{1,0:T(8,128)(2,1)S(1)}, bf16[64,4096]{1,0:T(8,128)(2,1)}, u32[]{:S(2)}) copy-start(bf16[64,4096]{1,0:T(8,128)(2,1)} %param.39) | copy-start | bytes 1572868
  312.8 318.0 %all-gather.22.cloned.1.call-start = ((), (), s32[]{:S(2)}) async-start(), calls=%async_computation.2 | async-start | bytes 1179648 | tf_op jit(solution)/shard_map/all_gather | solution.py:17
  313.6 6.0 copy-start.34
  313.6 6.0 copy-start.36
  313.6 7.2 copy-start.32
  313.6 350.6 %all-gather.26.cloned.1.call-start = ((), (), s32[]{:S(2)}) async-start(), calls=%async_computation.4 | async-start | bytes 1179648 | tf_op jit(solution)/shard_map/all_gather | solution.py:252
  324.3 21.4 %copy-start.14 = (f32[8,4,8,128]{3,2,1,0:T(8,128)}, f32[8,4,8,128]{3,2,1,0:T(8,128)S(1)}, u32[]{:S(2)}) copy-start(f32[8,4,8,128]{3,2,1,0:T(8,128)S(1)} %fusion.172) | copy-start | bytes 393220
  324.5 21.3 %copy-start.12 = (f32[64,4,128]{2,0,1:T(8,128)}, f32[64,4,128]{2,0,1:T(8,128)S(1)}, u32[]{:S(2)}) copy-start(f32[64,4,128]{2,0,1:T(8,128)S(1)} %get-tuple-element.1038) | copy-start | bytes 393220
  345.8 46.0 %copy-start.28 = (f32[512,4]{0,1:T(4,128)S(1)}, f32[512,4]{0,1:T(4,128)}, u32[]{:S(2)}) copy-start(f32[512,4]{0,1:T(4,128)} %get-tuple-element.1060) | copy-start | bytes 24580
  346.2 49.9 %copy-start.10 = (f32[512,4,128]{0,2,1:T(8,128)S(1)}, f32[512,4,128]{0,2,1:T(8,128)}, u32[]{:S(2)}) copy-start(f32[512,4,128]{0,2,1:T(8,128)} %get-tuple-element.1048) | copy-start | bytes 3145732
  348.5 318.5 %all-gather.24.cloned.1.call-start = ((), (), s32[]{:S(2)}) async-start(), calls=%async_computation.3 | async-start | bytes 1179648 | tf_op jit(solution)/shard_map/all_gather | solution.py:249
  349.6 381.0 %all-gather.34.cloned.1.call-start = ((), (), s32[]{:S(2)}) async-start(), calls=%async_computation.8 | async-start | bytes 1179648 | tf_op jit(solution)/shard_map/all_gather | solution.py:258
  350.6 27.0 %copy-start.13 = (f32[64,4,128]{2,0,1:T(8,128)}, f32[64,4,128]{2,0,1:T(8,128)S(1)}, u32[]{:S(2)}) copy-start(f32[64,4,128]{2,0,1:T(8,128)S(1)} %rev.39) | copy-start | bytes 393220
  381.8 351.7 %all-gather.32.cloned.1.call-start = ((), (), s32[]{:S(2)}) async-start(), calls=%async_computation.7 | async-start | bytes 1179648 | tf_op jit(solution)/shard_map/all_gather | solution.py:255
  382.9 365.3 %all-gather.28.cloned.1.call-start = ((), (), s32[]{:S(2)}) async-start(), calls=%async_computation.5 | async-start | bytes 1179648 | tf_op jit(solution)/shard_map/all_gather | solution.py:17
  402.0 15.3 %copy-start.39 = (pred[64,64]{1,0:T(8,128)(4,1)S(1)}, pred[64,64]{1,0:T(8,128)(4,1)}, u32[]{:S(2)}) copy-start(pred[64,64]{1,0:T(8,128)(4,1)} %copy-done.37) | copy-start | bytes 12292
  403.5 176.2 %copy-start.3 = (f32[4,512,128]{2,1,0:T(8,128)}, f32[4,512,128]{2,1,0:T(8,128)S(1)}, u32[]{:S(2)}) copy-start(f32[4,512,128]{2,1,0:T(8,128)S(1)} %copy.191) | copy-start | bytes 3145732
  621.9 126.3 %all-gather.30.cloned.1.call-start = ((), (), s32[]{:S(2)}) async-start(), calls=%async_computation.6 | async-start | bytes 1179648 | tf_op jit(solution)/shard_map/all_gather | solution.py:17
  623.7 210.6 %all-gather.18.cloned.1.call-start = ((), (), s32[]{:S(2)}) async-start(), calls=%async_computation | async-start | bytes 2621440 | tf_op jit(solution)/shard_map/all_gather | solution.py:304
  669.9 11.8 %copy-start.7 = (f32[4,128,128]{2,1,0:T(8,128)S(1)}, f32[4,128,128]{2,1,0:T(8,128)}, u32[]{:S(2)}) copy-start(f32[4,128,128]{2,1,0:T(8,128)} %get-tuple-element.610) | copy-start | bytes 786436
  812.1 22.3 %copy-start.46 = (f32[1024]{0:T(1024)S(1)}, f32[1024]{0:T(1024)}, u32[]{:S(2)}) copy-start(f32[1024]{0:T(1024)} %get-tuple-element.1034) | copy-start | bytes 12292
  834.4 6.5 copy-start.1
  (24 other events, 78.1 us)
Sparse Core Ops, SparseCore 0:
  312.9 37.7 all-gather.19
  352.8 39.7 all-gather.21
  394.7 39.3 all-gather.25
  436.1 39.5 all-gather.23
  477.6 39.9 all-gather.33
  519.6 39.5 all-gather.31
  622.0 37.5 all-gather.27
  661.8 39.0 all-gather.29
  814.4 19.8 all-gather.17
where the time goes:
time: 858 us; the launch traced here: 848 us
  other arithmetic  399 us (47%)
  matrix products  286 us (33%)
  local copies, waits for them, and re-layouts  74.3 us (9%)
  blocking collectives  49.8 us (6%)
  waiting for transfers between devices  20.3 us (2%)
  between operations  14.7 us (2%)
    another operation x7, other arithmetic, prepare_keys(): jax.scipy.linalg.solve_triangular(system, both_sides, lower=True, unit_di...  357 us
    dot_general x32, matrix products, compose(): jnp.einsum('hij,hjk->hik', second_map[0], first_map[1], precision=highest)  48.7 us
    psum x1, blocking collectives, body(): lax.psum((part_shift, part_scale, part_gate), 'sp')  39.4 us
    dot_general x9, matrix products, project(): jnp.dot(matrix, weight, preferred_element_type=jnp.float32)  30.8 us
    dot_general x18, matrix products, block_absorb(): jnp.einsum('hcd,hce->hde', late_in, new_in, precision=highest)  29.7 us
    dot_general x18, matrix products, block_absorb(): jnp.einsum('hcd,hce->hde', late_in, key_in, precision=highest)  27.3 us
    dot_general x16, matrix products, advance(): jnp.einsum('hcd,hce->hde', late_in, corrected, precision=highest)  24.6 us
    dot_general x16, matrix products, advance(): jnp.einsum('hcd,hde->hce', key_in, carried, precision=highest)  21.2 us
  transfers between devices with their start and end apart: 9, of which 1 were waited for; matrix products, arithmetic and copies ran while one was open for 51% of the time, Pallas kernels for 0%

commit v1 on v0

v1 whole, which is shorter than its diff:
```python
import functools

import jax
import jax.numpy as jnp
from jax import lax
from jax.experimental import pallas as pl
from jax.experimental.pallas import tpu as pltpu
from jax.sharding import PartitionSpec as P

HEAD_DIM = 128
CHUNK = 128
epsilon = 0.0001
bf16 = jnp.bfloat16
f32 = jnp.float32


def mm(a, b):
    return jnp.dot(a.astype(bf16), b.astype(bf16), preferred_element_type=f32)


def spans(tokens, ctx_tokens):
    size = min(CHUNK, tokens)
    lat = [(at, size) for at in range(0, tokens, size)]
    ctx_size = min(CHUNK, ctx_tokens)
    ctx = [(tokens + at, ctx_size) for at in range(0, ctx_tokens, ctx_size)]
    return lat, ctx


def prep_kernel(tokens, ctx_tokens, q_ref, k_ref, v_ref, col_ref, row_ref, o_ref, e_ref, map_ref):
    lat, ctx = spans(tokens, ctx_tokens)
    items = []
    shared = {}
    for at, size in lat + ctx:
        keys = k_ref[at : at + size, :]
        keys_t = keys.astype(f32).T
        gram = jnp.dot(keys, keys_t.astype(bf16), preferred_element_type=f32)
        rows = lax.broadcasted_iota(jnp.int32, (size, size), 0)
        cols = lax.broadcasted_iota(jnp.int32, (size, size), 1)
        diag = jnp.where(rows == cols, gram, 0.0)
        s_col = lax.rsqrt(jnp.sum(diag, axis=1, keepdims=True) + epsilon)
        s_row = lax.rsqrt(jnp.sum(diag, axis=0, keepdims=True) + epsilon)
        gram = gram * s_col * s_row
        entry = dict(keys=keys.astype(f32) * s_col, keys_t=keys_t * s_row, values=v_ref[at : at + size, :].astype(f32))
        if at < tokens:
            queries = q_ref[at : at + size, :].astype(f32)
            q_scale = lax.rsqrt(jnp.sum(queries * queries, axis=1, keepdims=True) + epsilon) * HEAD_DIM**-0.5
            entry["queries"] = queries * q_scale
            entry["score"] = (
                jnp.dot(q_ref[at : at + size, :], keys_t.astype(bf16), preferred_element_type=f32) * q_scale * s_row
            )
        shared[at] = entry
        for d in range(2):
            rate_col = col_ref[0, at : at + size, 2 * d : 2 * d + 1]
            run_col = col_ref[0, at : at + size, 2 * d + 1 : 2 * d + 2]
            run_row = row_ref[0, 2 * d + 1 : 2 * d + 2, at : at + size]
            inside = rows >= cols if d == 0 else rows <= cols
            strict = rows > cols if d == 0 else rows < cols
            decay = jnp.where(inside, jnp.exp(jnp.minimum(run_col - run_row, 0.0)), 0.0)
            system = jnp.where(strict, gram * decay * rate_col, 0.0)
            item = dict(at=at, size=size, d=d, rate_col=rate_col, run_col=run_col, run_row=run_row)
            item["system"] = system
            if at < tokens:
                item["score"] = entry["score"] * decay
            near = (rows // 2) == (cols // 2)
            item["inv"] = jnp.where(rows == cols, 1.0, jnp.where(near, -system, 0.0))
            items.append(item)
    span = 2
    while span < max(item["size"] for item in items):
        firsts = []
        for item in items:
            if span >= item["size"]:
                firsts.append(None)
                continue
            size = item["size"]
            rows = lax.broadcasted_iota(jnp.int32, (size, size), 0) // span
            cols = lax.broadcasted_iota(jnp.int32, (size, size), 1) // span
            if item["d"] == 0:
                mask = ((rows % 2) == 1) & (cols == rows - 1)
            else:
                mask = ((cols % 2) == 1) & (rows == cols - 1)
            firsts.append(mm(jnp.where(mask, item["system"], 0.0), item["inv"]))
        for item, first in zip(items, firsts):
            if first is not None:
                item["inv"] = item["inv"] - mm(item["inv"], first)
        span *= 2
    for item in items:
        entry = shared[item["at"]]
        growth = jnp.exp(item["run_col"])
        both = jnp.concatenate(
            [entry["values"] * item["rate_col"], entry["keys"] * (item["rate_col"] * growth)], axis=1
        )
        item["solved"] = mm(item["inv"], both)
        last = item["run_row"][:, item["size"] - 1 :] if item["d"] == 0 else item["run_row"][:, :1]
        item["gate"] = jnp.exp(last)
        late_t = entry["keys_t"] * jnp.exp(last - item["run_row"])
        item["late"] = mm(late_t, item["solved"])
        if item["at"] < tokens:
            weighed = mm(item["score"], item["solved"])
            item["local"] = weighed[:, :HEAD_DIM]
            item["early"] = entry["queries"] * growth - weighed[:, HEAD_DIM:]
    eye_r = lax.broadcasted_iota(jnp.int32, (HEAD_DIM, HEAD_DIM), 0)
    eye_c = lax.broadcasted_iota(jnp.int32, (HEAD_DIM, HEAD_DIM), 1)
    eye = (eye_r == eye_c).astype(f32)

    def chain(chunks, d, emit):
        carry = None
        for item in chunks if d == 0 else chunks[::-1]:
            if emit:
                if carry is None:
                    out, early = item["local"], item["early"]
                else:
                    moved = mm(item["early"], carry)
                    out = item["local"] + moved[:, :HEAD_DIM]
                    early = item["early"] + moved[:, HEAD_DIM:]
                e_ref[0, item["at"] : item["at"] + item["size"], d * HEAD_DIM : (d + 1) * HEAD_DIM] = early.astype(
                    bf16
                )
                item["out"] = out
            late, gate = item["late"], item["gate"]
            fresh = jnp.concatenate([late[:, :HEAD_DIM], (gate - 1.0) * eye - late[:, HEAD_DIM:]], axis=1)
            if carry is None:
                carry = fresh
            else:
                carry = gate * carry + fresh - mm(late[:, HEAD_DIM:], carry)
        return carry

    for d in range(2):
        latents = [i for i in items if i["d"] == d and i["at"] < tokens]
        contexts = [i for i in items if i["d"] == d and i["at"] >= tokens]
        map_ref[0, d, 0] = chain(contexts, d, False).astype(bf16)
        map_ref[0, d, 1] = chain(latents, d, True).astype(bf16)
    for at, size in lat:
        pair = [i for i in items if i["at"] == at]
        o_ref[0, at : at + size, :] = pair[0]["out"] + pair[1]["out"]


def prepare(queries, keys, values, col, row, tokens, ctx_tokens):
    heads = col.shape[0]
    every = tokens + ctx_tokens
    return pl.pallas_call(
        functools.partial(prep_kernel, tokens, ctx_tokens),
        grid=(heads,),
        in_specs=[
            pl.BlockSpec((tokens, HEAD_DIM), lambda h: (0, h)),
            pl.BlockSpec((every, HEAD_DIM), lambda h: (0, h)),
            pl.BlockSpec((every, HEAD_DIM), lambda h: (0, h)),
            pl.BlockSpec((1, every, col.shape[2]), lambda h: (h, 0, 0)),
            pl.BlockSpec((1, row.shape[1], every), lambda h: (h, 0, 0)),
        ],
        out_specs=[
            pl.BlockSpec((1, tokens, HEAD_DIM), lambda h: (h, 0, 0)),
            pl.BlockSpec((1, tokens, 2 * HEAD_DIM), lambda h: (h, 0, 0)),
            pl.BlockSpec((1, 2, 2, HEAD_DIM, 2 * HEAD_DIM), lambda h: (h, 0, 0, 0, 0)),
        ],
        out_shape=[
            jax.ShapeDtypeStruct((heads, tokens, HEAD_DIM), f32),
            jax.ShapeDtypeStruct((heads, tokens, 2 * HEAD_DIM), bf16),
            jax.ShapeDtypeStruct((heads, 2, 2, HEAD_DIM, 2 * HEAD_DIM), bf16),
        ],
        compiler_params=pltpu.CompilerParams(vmem_limit_bytes=60 * 1024 * 1024),
        name="prepare",
    )(queries, keys, values, col, row)


def apply_maps(maps, state):
    high = state.astype(bf16)
    low = (state - high.astype(f32)).astype(bf16)
    move = maps[:, HEAD_DIM:]
    return (
        state
        + maps[:, :HEAD_DIM].astype(f32)
        + jnp.dot(move, high, preferred_element_type=f32)
        + jnp.dot(move, low, preferred_element_type=f32)
    )


def chain_kernel(peers, per, maps_ref, start_ref):
    place = lax.axis_index("sp")
    for slot in range(per):
        back = lax.rem(place * per + slot, 2)

        def at(step):
            return step + back * (peers - 1 - 2 * step)

        state = jnp.zeros((HEAD_DIM, HEAD_DIM), f32)
        for step in range(peers):
            state = apply_maps(maps_ref[at(step), slot, 0], state)
        for step in range(peers):
            start_ref[at(step), slot] = state.astype(bf16)
            if step < peers - 1:
                state = apply_maps(maps_ref[at(step), slot, 1], state)


def finish_kernel(o_ref, e_ref, s_ref, gain_ref, out_ref):
    states = s_ref[...].reshape(2 * HEAD_DIM, HEAD_DIM)
    combined = o_ref[0] + jnp.dot(e_ref[0], states, preferred_element_type=f32)
    scale = lax.rsqrt(jnp.mean(combined * combined, axis=1, keepdims=True) + epsilon)
    out_ref[...] = (combined * scale * gain_ref[...]).astype(bf16)


def finish(local, early, starts, gain):
    heads, tokens, _ = local.shape
    return pl.pallas_call(
        finish_kernel,
        grid=(heads,),
        in_specs=[
            pl.BlockSpec((1, tokens, HEAD_DIM), lambda h: (h, 0, 0)),
            pl.BlockSpec((1, tokens, 2 * HEAD_DIM), lambda h: (h, 0, 0)),
            pl.BlockSpec((2, HEAD_DIM, HEAD_DIM), lambda h: (h, 0, 0)),
            pl.BlockSpec((1, HEAD_DIM), lambda h: (0, 0)),
        ],
        out_specs=pl.BlockSpec((tokens, HEAD_DIM), lambda h: (0, h)),
        out_shape=jax.ShapeDtypeStruct((tokens, heads * HEAD_DIM), bf16),
        name="finish",
    )(local, early, starts, gain)


def start_states(maps):
    items = maps.shape[0]
    peers = lax.axis_size("sp")
    per = -(-items // peers)
    padded = jnp.pad(maps, ((0, per * peers - items), (0, 0), (0, 0), (0, 0)))
    padded = padded.reshape((peers, per) + maps.shape[1:])
    mine = lax.all_to_all(padded, "sp", 0, 0)
    starts = pl.pallas_call(
        functools.partial(chain_kernel, peers, per),
        out_shape=jax.ShapeDtypeStruct((peers, per, HEAD_DIM, HEAD_DIM), bf16),
        name="chain",
    )(mine)
    back = lax.all_to_all(starts, "sp", 0, 0)
    return back.reshape(peers * per, HEAD_DIM, HEAD_DIM)[:items]


def rms_rows(row_data, row_gain):
    values = row_data.astype(f32)
    scaled = values * lax.rsqrt(jnp.mean(values * values, axis=-1, keepdims=True) + epsilon)
    return scaled * row_gain


def project(matrix, weight):
    return jnp.dot(matrix, weight, preferred_element_type=f32).astype(bf16)


def running_sums(log_decay, size):
    parts = log_decay.reshape((-1, size) + log_decay.shape[1:])
    lower = jnp.tril(jnp.ones((size, size), f32))
    ahead = jnp.einsum("ij,njh->nih", lower, parts[:, :, 0], precision=lax.Precision.HIGHEST)
    behind = jnp.einsum("ji,njh->nih", lower, parts[:, :, 1], precision=lax.Precision.HIGHEST)
    return jnp.stack([ahead, behind], axis=2).reshape(log_decay.shape)


def body(
    latent,
    context,
    condition,
    context_condition,
    shift_weight,
    scale_weight,
    gate_weight,
    norm_gain,
    query_weight,
    key_weight,
    value_weight,
    write_weight,
    decay_weight,
    write_bias,
    decay_bias,
    log_rate,
    head_gain,
    out_weight,
):
    heads_here = query_weight.shape[1] // HEAD_DIM
    first_head = lax.axis_index("tp") * heads_here
    own_cols = gate_weight.shape[1]
    col_start = lax.axis_index("tp") * own_cols
    tokens, ctx_tokens = latent.shape[0], context.shape[0]
    stacked = jnp.stack([condition, context_condition]).astype(f32)
    silu_rows = jax.nn.silu(stacked).astype(bf16)
    partial_rows = jnp.concatenate(
        [
            jnp.dot(silu_rows, shift_weight, preferred_element_type=f32),
            jnp.dot(silu_rows, scale_weight, preferred_element_type=f32),
            jnp.dot(silu_rows[:1], gate_weight, preferred_element_type=f32),
        ],
        axis=0,
    )
    summed = jnp.sum(lax.all_gather(partial_rows, "sp"), axis=0)
    gate_row = summed[4]
    rows = lax.all_gather(summed[:4], "tp", axis=1, tiled=True)

    def modulate(row_data, row_index):
        normed = rms_rows(row_data, norm_gain)
        return (normed * (1.0 + rows[2 + row_index]) + rows[row_index]).astype(bf16)

    modulated = jnp.concatenate([modulate(latent, 0), modulate(context, 1)], axis=0)

    def own_heads(array):
        return lax.dynamic_slice_in_dim(array, first_head, heads_here, array.ndim - 1)

    gate_weights = jnp.concatenate(
        [
            own_heads(write_weight).reshape(write_weight.shape[0], -1),
            own_heads(decay_weight).reshape(decay_weight.shape[0], -1),
        ],
        axis=1,
    )
    queries = project(modulated, query_weight)
    keys = project(modulated, key_weight)
    values = project(modulated, value_weight)
    pre = project(modulated, gate_weights).astype(f32).reshape(-1, 2, 2, heads_here)
    rate = jax.nn.sigmoid(pre[:, 0] + own_heads(write_bias))
    log_decay = -jnp.exp(own_heads(log_rate)) * jax.nn.softplus(pre[:, 1] + own_heads(decay_bias))
    lat, ctx = spans(tokens, ctx_tokens)
    running = jnp.concatenate(
        [running_sums(log_decay[:tokens], lat[0][1]), running_sums(log_decay[tokens:], ctx[0][1])], axis=0
    )
    gates = jnp.stack([rate, running], axis=2)
    col = jnp.transpose(gates, (3, 0, 1, 2)).reshape(heads_here, tokens + ctx_tokens, 4)
    row = jnp.transpose(gates, (3, 1, 2, 0)).reshape(heads_here, 4, tokens + ctx_tokens)
    local, early, maps = prepare(queries, keys, values, col, row, tokens, ctx_tokens)
    starts = start_states(maps.reshape((heads_here * 2, 2) + maps.shape[3:]))
    head_out = finish(local, early, starts, head_gain[None, :])
    branch = jnp.dot(
        lax.all_gather(head_out, "tp", axis=1, tiled=True), out_weight, preferred_element_type=f32
    )
    residual = lax.dynamic_slice_in_dim(latent, col_start, own_cols, 1).astype(f32)
    return (residual + gate_row * branch).astype(bf16)


def solution(mesh):
    placed = (
        P("sp", None),
        P("sp", None),
        P("sp"),
        P("sp"),
        P("sp", "tp"),
        P("sp", "tp"),
        P("sp", "tp"),
        P(),
        P(None, "tp"),
        P(None, "tp"),
        P(None, "tp"),
        P(),
        P(),
        P(),
        P(),
        P(),
        P(),
        P(None, "tp"),
    )
    return jax.shard_map(body, mesh=mesh, in_specs=placed, out_specs=P("sp", "tp"), check_vma=False)
```

time: 858 us -> 188 us (0.22); the launches traced: 848 us -> 188 us
  other arithmetic: 399 us -> 9.29 us
  matrix products: 286 us -> 23 us
  local copies, waits for them, and re-layouts: 74.3 us -> 6.69 us
  blocking collectives: 49.8 us -> 82.4 us
  Pallas kernels: 0 us -> 30.8 us
    another operation x11 -> x1, other arithmetic: 361 us -> 0.01 us  [body(): gates = jnp.stack([rate, running], axis=2)]
    dot_general x204 -> x11, matrix products: 274 us -> 16.6 us  [the longest x4 15.2 us: project(): return jnp.dot(matrix, weight, preferred_element_type=f32).astype(bf16)]
    all_to_all x0 -> x2, blocking collectives: none -> 44.6 us  [the longest x1 31.9 us: start_states(): mine = lax.all_to_all(padded, 'sp', 0, 0)]
    psum x1 -> x0, blocking collectives: 39.4 us -> none  [body(): lax.psum((part_shift, part_scale, part_gate), 'sp')]
    pallas_call x0 -> x3, Pallas kernels: none -> 30.8 us  [the longest x1 22.6 us: prepare(): pl.pallas_call(functools.partial(prep_kernel, tokens, ctx_tokens), grid=(...]
    all_gather x2, blocking collectives: 10.3 us -> 37.8 us  [the longest x1 32.6 us: body(): summed = jnp.sum(lax.all_gather(partial_rows, 'sp'), axis=0)]
    rev x9 -> x0, local copies, waits for them, and re-layouts: 18.9 us -> none  [the longest x1 8.84 us: body(): jnp.flip(value_vecs, 0)]
    convert_element_type x12 -> x3, other arithmetic: 19.6 us -> 4.36 us  [the longest x2 4.34 us: modulate(): return (normed * (1.0 + rows[2 + row_index]) + rows[row_index]).astype(bf16)]
  transfers between devices with their start and end apart: 9 -> 1, of which waited for: 1 -> 1; matrix products, arithmetic and copies ran while one was open for 51% -> 0% of each run, Pallas kernels for 0% -> 0%
where the time goes in v1:
time: 188 us
  blocking collectives  82.4 us (44%)
  Pallas kernels  30.8 us (16%)
  matrix products  23 us (12%)
  waiting for transfers between devices  21.7 us (12%)
  between operations  13.6 us (7%)
  other arithmetic  9.29 us (5%)
  local copies, waits for them, and re-layouts  6.69 us (4%)
    all_gather x1, blocking collectives, body(): summed = jnp.sum(lax.all_gather(partial_rows, 'sp'), axis=0)  32.6 us
    all_to_all x1, blocking collectives, start_states(): mine = lax.all_to_all(padded, 'sp', 0, 0)  31.9 us
    pallas_call x1, Pallas kernels, prepare(): pl.pallas_call(functools.partial(prep_kernel, tokens, ctx_tokens), grid=(...  22.6 us
    all_gather x1, waiting for transfers between devices, body(): lax.all_gather(head_out, 'tp', axis=1, tiled=True)  21.7 us
    dot_general x4, matrix products, project(): return jnp.dot(matrix, weight, preferred_element_type=f32).astype(bf16)  15.2 us
    all_to_all x1, blocking collectives, start_states(): back = lax.all_to_all(starts, 'sp', 0, 0)  12.7 us
    dot_general x1, matrix products, body(): jnp.dot(lax.all_gather(head_out, 'tp', axis=1, tiled=True), out_weight, p...  6.4 us
    all_gather x1, blocking collectives, body(): rows = lax.all_gather(summed[:4], 'tp', axis=1, tiled=True)  5.24 us
  transfers between devices with their start and end apart: 1, of which 1 were waited for; matrix products, arithmetic and copies ran while one was open for 0% of the time, Pallas kernels for 0%

profile of v1, /device:TPU:0, one launch (start us, length us, event | category | flops | bytes accessed | tf_op | source)
XLA Modules:
  0.0 187.6 jit_solution(10424750037130479756)
XLA Ops:
  6.6 1.4 fusion.6
  8.0 0.7 stack.34
  8.7 0.7 stack.35
  9.4 3.1 %fusion = f32[512]{0:T(512)S(1)} fusion(bf16[512,4096]{1,0:T(8,128)(2,1)} %param.18), kind=kLoop, calls=%fused_computation.2 | loop fusion | flops 6290944 | bytes 4196352 | tf_op jit(solution)/shard_map/reduce_sum | solution.py:236
  12.5 0.2 fusion.40
  12.8 0.2 fusion.53
  13.0 0.3 fusion.52
  13.4 1.1 constant_dynamic-slice_fusion.3
  14.5 32.6 %all-gather.1 = f32[8,5,1024]{2,1,0:T(8,128)S(1)} all-gather(f32[1,5,1024]{2,1,0:T(8,128)S(1)} %maximum_bitcast_fusion), channel_id=2, replica_groups=mesh['sp'=8,'tp'=4] {'sp'}, dimensions={0}, use_global_device_ids=true | all-gather | bytes 184320 | tf_op jit(solution)/shard_map/all_gather | solution.py:287
  47.1 5.2 %all_gather.14 = f32[4,4096]{1,0:T(4,128)S(1)} all-gather(f32[4,1024]{1,0:T(4,128)S(1)} %slice.62), channel_id=1, replica_groups=mesh['sp'=8,'tp'=4] {'tp'}, dimensions={1}, use_global_device_ids=true | all-gather | bytes 81920 | tf_op jit(solution)/shard_map/all_gather | solution.py:289
  52.4 0.3 fusion.10
  52.7 4.1 %fusion.4 = bf16[512,4096]{1,0:T(8,128)(2,1)S(1)} fusion(bf16[512,4096]{1,0:T(8,128)(2,1)} %param.18, f32[4096]{0:T(1024)S(1)} %bitcast.102, f32[4096]{0:T(1024)S(1)} %bitcast.101, f32[4096]{0:T(1024)S(1)} %copy-done.6, f32[512]{0:T(512)S(1)} %add_rsqrt_fusion), kind=kLoop, calls=%fused_computation.6 | loop fusion | flops 12582912 | bytes 8439808 | tf_op jit(solution)/shard_map/convert_element_type | solution.py:293
  56.8 1.9 %copy-done.1 = bf16[512,4096]{1,0:T(8,128)(2,1)} copy-done((bf16[512,4096]{1,0:T(8,128)(2,1)}, bf16[512,4096]{1,0:T(8,128)(2,1)S(1)}, u32[]{:S(2)}) %copy-start.1) | copy-done | bytes 4194328
  58.7 1.3 fusion.5
  60.2 0.1 fusion.26
  60.3 0.1 convolution_bitcast_fusion.2
  60.4 0.2 convolution_bitcast_fusion.3
  60.6 0.2 convolution_bitcast_fusion
  60.8 0.2 convolution_bitcast_fusion.1
  61.0 0.1 fusion.32
  61.2 0.7 reshape.107.row_ref
  61.9 7.0 %convolution_convert_fusion.1.k_ref = bf16[576,512]{1,0:T(8,128)(2,1)} fusion(bf16[4096,512]{1,0:T(8,128)(2,1)} %param.27, bf16[64,4096]{1,0:T(8,128)(2,1)S(1)} %fusion.10, bf16[512,4096]{1,0:T(8,128)(2,1)} %copy-done.1), kind=kOutput, calls=%fused_computation.10 | convolution fusion | flops 2425651200 | bytes 9502720 | tf_op jit(solution)/shard_map/dot_general | solution.py:241
  68.9 3.4 %convolution_convert_fusion.v_ref = bf16[576,512]{1,0:T(8,128)(2,1)} fusion(bf16[4096,512]{1,0:T(8,128)(2,1)S(1)} %copy-done.10, bf16[64,4096]{1,0:T(8,128)(2,1)S(1)} %fusion.10, bf16[512,4096]{1,0:T(8,128)(2,1)S(1)} %copy-done.2), kind=kOutput, calls=%fused_computation.9 | convolution fusion | flops 2425651200 | bytes 9502720 | tf_op jit(solution)/shard_map/dot_general | solution.py:241
  72.3 3.4 %convolution_convert_fusion.2.q_ref = bf16[576,512]{1,0:T(8,128)(2,1)} fusion(bf16[4096,512]{1,0:T(8,128)(2,1)S(1)} %copy-done.11, bf16[64,4096]{1,0:T(8,128)(2,1)S(1)} %fusion.10, bf16[512,4096]{1,0:T(8,128)(2,1)S(1)} %copy-done.2), kind=kOutput, calls=%fused_computation.11 | convolution fusion | flops 2425651200 | bytes 9502720 | tf_op jit(solution)/shard_map/dot_general | solution.py:241
  75.7 1.4 copy.30.col_ref
  77.2 22.6 %prepare.1 = (f32[4,512,128]{2,1,0:T(8,128)}, bf16[4,512,256]{2,1,0:T(8,128)(2,1)}, bf16[4,2,2,128,256]{4,3,2,1,0:T(8,128)(2,1)}) custom-call(bf16[576,512]{1,0:T(8,128)(2,1)} %convolution_convert_fusion.2.q_ref, bf16[576,512]{1,0:T(8,128)(2,1)} %convolution_convert_fusion.1.k_ref, bf16[576,512]{1,0:T(8,128)(2,1)} %convolution_convert_fusion.v_ref, ...), custom_call_target="tpu_custom_call" | custom-call | tf_op jit(solution)/shard_map/prepare/pallas_call | solution.py:140
  99.7 31.9 %all_to_all.10.maps_ref = bf16[8,1,2,128,256]{4,3,2,1,0:T(8,128)(2,1)} all-to-all(bf16[8,1,2,128,256]{4,3,2,1,0:T(8,128)(2,1)} %bitcast.99), channel_id=1, replica_groups=mesh['sp'=8,'tp'=4] {'sp'}, dimensions={0} | all-to-all | bytes 2097152 | tf_op jit(solution)/shard_map/all_to_all | solution.py:224
  131.6 4.2 %chain.1 = bf16[8,1,128,128]{3,2,1,0:T(8,128)(2,1)} custom-call(bf16[8,1,2,128,256]{4,3,2,1,0:T(8,128)(2,1)} %all_to_all.10.maps_ref), custom_call_target="tpu_custom_call" | custom-call | tf_op jit(solution)/shard_map/chain/pallas_call | solution.py:225
  135.8 12.7 %all_to_all.11 = bf16[8,1,128,128]{3,2,1,0:T(8,128)(2,1)} all-to-all(bf16[8,1,128,128]{3,2,1,0:T(8,128)(2,1)} %chain.1), channel_id=1, replica_groups=mesh['sp'=8,'tp'=4] {'sp'}, dimensions={0} | all-to-all | bytes 524288 | tf_op jit(solution)/shard_map/all_to_all | solution.py:230
  148.5 4.1 %finish.1 = bf16[512,512]{1,0:T(8,128)(2,1)} custom-call(f32[4,512,128]{2,1,0:T(8,128)} %get-tuple-element.8.o_ref, bf16[4,512,256]{2,1,0:T(8,128)(2,1)} %get-tuple-element.9.e_ref, bf16[8,128,128]{2,1,0:T(8,128)(2,1)} %bitcast.98, f32[1,128]{1,0:T(1,128)} %bitcast.106), custom_call_target="tpu_custom_call" | custom-call | tf_op jit(solution)/shard_map/finish/pallas_call | solution.py:203
  152.6 21.7 %all-gather.4.cloned.1.call-done = bf16[512,2048]{1,0:T(8,128)(2,1)} async-done(((bf16[512,512]{1,0:T(8,128)(2,1)}), bf16[512,2048]{1,0:T(8,128)(2,1)}) %all-gather.4.cloned.1.call-update) | async-done | bytes 2097168 | tf_op jit(solution)/shard_map/all_gather | solution.py:324
  174.3 6.4 %add_convert_fusion = bf16[512,1024]{1,0:T(8,128)(2,1)} fusion(bf16[512,2048]{1,0:T(8,128)(2,1)} %all-gather.4.cloned.1.call-done, bf16[2048,1024]{1,0:T(8,128)(2,1)} %param.35, f32[1024]{0:T(1024)S(1)} %bitcast.105, bf16[512,4096]{1,0:T(8,128)(2,1)} %param.18, s32[]{:T(128)S(6)} %select_n.26), kind=kOutput, calls=%fused_computation.8 | convolution fusion | flops 2149580800 | bytes 8392708 | tf_op jit(solution)/shard_map/dot_general | solution.py:323
  (45 shorter events, 0.5 us)
Async XLA Ops:
  6.5 6.3 %copy-start = (bf16[512,1024]{1,0:T(8,128)(2,1)S(1)}, bf16[512,1024]{1,0:T(8,128)(2,1)}, u32[]{:S(2)}) copy-start(bf16[512,1024]{1,0:T(8,128)(2,1)} %param.23) | copy-start | bytes 3145732
  6.5 6.0 %copy-start.4 = (bf16[512,1024]{1,0:T(8,128)(2,1)S(1)}, bf16[512,1024]{1,0:T(8,128)(2,1)}, u32[]{:S(2)}) copy-start(bf16[512,1024]{1,0:T(8,128)(2,1)} %param.24) | copy-start | bytes 3145732
  6.5 6.8 %copy-start.7 = (f32[2,16]{1,0:T(2,128)S(1)}, f32[2,16]{1,0:T(2,128)}, u32[]{:S(2)}) copy-start(f32[2,16]{1,0:T(2,128)} %param.33) | copy-start | bytes 388
  6.5 167.8 %all-gather.4.cloned.1.call-start = ((), (), s32[]{:S(2)}) async-start(), calls=%async_computation.2 | async-start | bytes 2621440 | tf_op jit(solution)/shard_map/all_gather | solution.py:324
  6.6 6.5 %copy-start.5 = (bf16[512,1024]{1,0:T(8,128)(2,1)S(1)}, bf16[512,1024]{1,0:T(8,128)(2,1)}, u32[]{:S(2)}) copy-start(bf16[512,1024]{1,0:T(8,128)(2,1)} %param.22) | copy-start | bytes 3145732
  9.3 43.0 %copy-start.3 = (bf16[64,4096]{1,0:T(8,128)(2,1)S(1)}, bf16[64,4096]{1,0:T(8,128)(2,1)}, u32[]{:S(2)}) copy-start(bf16[64,4096]{1,0:T(8,128)(2,1)} %param.19) | copy-start | bytes 1572868
  9.4 43.1 %copy-start.6 = (f32[4096]{0:T(1024)S(1)}, f32[4096]{0:T(1024)}, u32[]{:S(2)}) copy-start(f32[4096]{0:T(1024)} %param.25) | copy-start | bytes 49156
  56.8 2.0 %copy-start.1 = (bf16[512,4096]{1,0:T(8,128)(2,1)}, bf16[512,4096]{1,0:T(8,128)(2,1)S(1)}, u32[]{:S(2)}) copy-start(bf16[512,4096]{1,0:T(8,128)(2,1)S(1)} %fusion.4) | copy-start | bytes 12582916
  58.7 1.4 copy-start.8
  58.7 1.4 copy-start.9
  61.9 7.0 %copy-start.2 = (bf16[512,4096]{1,0:T(8,128)(2,1)S(1)}, bf16[512,4096]{1,0:T(8,128)(2,1)}, u32[]{:S(2)}) copy-start(bf16[512,4096]{1,0:T(8,128)(2,1)} %copy-done.1) | copy-start | bytes 12582916
  61.9 7.0 %copy-start.10 = (bf16[4096,512]{1,0:T(8,128)(2,1)S(1)}, bf16[4096,512]{1,0:T(8,128)(2,1)}, u32[]{:S(2)}) copy-start(bf16[4096,512]{1,0:T(8,128)(2,1)} %param.28) | copy-start | bytes 12582916
  68.9 3.4 %copy-start.11 = (bf16[4096,512]{1,0:T(8,128)(2,1)S(1)}, bf16[4096,512]{1,0:T(8,128)(2,1)}, u32[]{:S(2)}) copy-start(bf16[4096,512]{1,0:T(8,128)(2,1)} %param.26) | copy-start | bytes 12582916
Sparse Core Ops, SparseCore 0:
  152.7 21.5 all-gather.3

commit v2 on v1

--- a/solution.py
+++ b/solution.py
@@ -127,8 +127,8 @@
     for d in range(2):
         latents = [i for i in items if i["d"] == d and i["at"] < tokens]
         contexts = [i for i in items if i["d"] == d and i["at"] >= tokens]
-        map_ref[0, d, 0] = chain(contexts, d, False).astype(bf16)
-        map_ref[0, d, 1] = chain(latents, d, True).astype(bf16)
+        map_ref[0, d] = chain(contexts, d, False).astype(bf16)
+        map_ref[1, d] = chain(latents, d, True).astype(bf16)
     for at, size in lat:
         pair = [i for i in items if i["at"] == at]
         o_ref[0, at : at + size, :] = pair[0]["out"] + pair[1]["out"]
@@ -150,12 +150,12 @@
         out_specs=[
             pl.BlockSpec((1, tokens, HEAD_DIM), lambda h: (h, 0, 0)),
             pl.BlockSpec((1, tokens, 2 * HEAD_DIM), lambda h: (h, 0, 0)),
-            pl.BlockSpec((1, 2, 2, HEAD_DIM, 2 * HEAD_DIM), lambda h: (h, 0, 0, 0, 0)),
+            pl.BlockSpec((2, 2, HEAD_DIM, 2 * HEAD_DIM), lambda h: (0, h, 0, 0)),
         ],
         out_shape=[
             jax.ShapeDtypeStruct((heads, tokens, HEAD_DIM), f32),
             jax.ShapeDtypeStruct((heads, tokens, 2 * HEAD_DIM), bf16),
-            jax.ShapeDtypeStruct((heads, 2, 2, HEAD_DIM, 2 * HEAD_DIM), bf16),
+            jax.ShapeDtypeStruct((2, 2 * heads, HEAD_DIM, 2 * HEAD_DIM), bf16),
         ],
         compiler_params=pltpu.CompilerParams(vmem_limit_bytes=60 * 1024 * 1024),
         name="prepare",
@@ -174,61 +174,195 @@
     )
 
 
-def chain_kernel(peers, per, maps_ref, start_ref):
-    place = lax.axis_index("sp")
-    for slot in range(per):
-        back = lax.rem(place * per + slot, 2)
-
-        def at(step):
-            return step + back * (peers - 1 - 2 * step)
-
-        state = jnp.zeros((HEAD_DIM, HEAD_DIM), f32)
-        for step in range(peers):
-            state = apply_maps(maps_ref[at(step), slot, 0], state)
-        for step in range(peers):
-            start_ref[at(step), slot] = state.astype(bf16)
-            if step < peers - 1:
-                state = apply_maps(maps_ref[at(step), slot, 1], state)
-
-
-def finish_kernel(o_ref, e_ref, s_ref, gain_ref, out_ref):
-    states = s_ref[...].reshape(2 * HEAD_DIM, HEAD_DIM)
-    combined = o_ref[0] + jnp.dot(e_ref[0], states, preferred_element_type=f32)
-    scale = lax.rsqrt(jnp.mean(combined * combined, axis=1, keepdims=True) + epsilon)
-    out_ref[...] = (combined * scale * gain_ref[...]).astype(bf16)
-
-
-def finish(local, early, starts, gain):
+def on_mesh(sp=None, tp=None):
+    return (lax.axis_index("sp") if sp is None else sp, lax.axis_index("tp") if tp is None else tp)
+
+
+def send(src, dst, send_sem, recv_sem, device):
+    return pltpu.make_async_remote_copy(
+        src_ref=src,
+        dst_ref=dst,
+        send_sem=send_sem,
+        recv_sem=recv_sem,
+        device_id=device,
+        device_id_type=pl.DeviceIdType.MESH,
+    )
+
+
+def greet(devices):
+    barrier = pltpu.get_barrier_semaphore()
+    for device in devices:
+        pl.semaphore_signal(barrier, inc=1, device_id=device, device_id_type=pl.DeviceIdType.MESH)
+
+
+def modulation_kernel(
+    sp, tp, silu_ref, shift_ref, scale_ref, gate_ref, rows_ref, gate_out, got, blocks, sent_a, recv_a, sent_b, recv_b
+):
+    me, col = lax.axis_index("sp"), lax.axis_index("tp")
+    width = shift_ref.shape[1]
+    rings = [on_mesh(sp=lax.rem(me + r, sp)) for r in range(1, sp)]
+    cross = [on_mesh(tp=lax.rem(col + r, tp)) for r in range(1, tp)]
+    greet(rings + cross)
+    silu = silu_ref[...]
+    shift = jnp.dot(silu, shift_ref[...], preferred_element_type=f32)
+    scale = jnp.dot(silu, scale_ref[...], preferred_element_type=f32)
+    gate = jnp.dot(silu, gate_ref[...], preferred_element_type=f32)
+    got[me] = jnp.concatenate([shift[0:2], scale[0:2], gate[0:1], jnp.zeros((3, width), f32)], axis=0)
+    pl.semaphore_wait(pltpu.get_barrier_semaphore(), len(rings) + len(cross))
+    out = []
+    for r, device in enumerate(rings):
+        out.append(send(got.at[me], got.at[me], sent_a.at[r], recv_a.at[me], device))
+        out[-1].start()
+    for r in range(1, sp):
+        src = lax.rem(me + r, sp)
+        send(got.at[src], got.at[src], sent_a.at[0], recv_a.at[src], on_mesh(sp=src)).wait_recv()
+    total = got[0]
+    for place in range(1, sp):
+        total = total + got[place]
+    blocks[col] = total
+    gate_out[...] = total[4:5]
+    for r, device in enumerate(cross):
+        out.append(send(blocks.at[col], blocks.at[col], sent_b.at[r], recv_b.at[col], device))
+        out[-1].start()
+    for r in range(1, tp):
+        src = lax.rem(col + r, tp)
+        send(blocks.at[src], blocks.at[src], sent_b.at[0], recv_b.at[src], on_mesh(tp=src)).wait_recv()
+    for place in range(tp):
+        rows_ref[:, place * width : (place + 1) * width] = blocks[place][0:4]
+    for copy in out:
+        copy.wait_send()
+
+
+def modulation(silu_rows, shift_weight, scale_weight, gate_weight):
+    sp, tp = lax.axis_size("sp"), lax.axis_size("tp")
+    width = shift_weight.shape[1]
+    vmem = pl.BlockSpec(memory_space=pltpu.VMEM)
+    return pl.pallas_call(
+        functools.partial(modulation_kernel, sp, tp),
+        in_specs=[vmem] * 4,
+        out_specs=[vmem] * 2,
+        out_shape=[jax.ShapeDtypeStruct((4, tp * width), f32), jax.ShapeDtypeStruct((1, width), f32)],
+        scratch_shapes=[
+            pltpu.VMEM((sp, 8, width), f32),
+            pltpu.VMEM((tp, 8, width), f32),
+            pltpu.SemaphoreType.DMA((sp,)),
+            pltpu.SemaphoreType.DMA((sp,)),
+            pltpu.SemaphoreType.DMA((tp,)),
+            pltpu.SemaphoreType.DMA((tp,)),
+        ],
+        compiler_params=pltpu.CompilerParams(collective_id=0, has_side_effects=True),
+        name="modulation",
+    )(jnp.pad(silu_rows, ((0, 6), (0, 0))), shift_weight, scale_weight, gate_weight)
+
+
+def exchange_kernel(
+    sp, per, maps_ref, o_ref, e_ref, gain_ref, out_ref, got, starts, back, sent_a, recv_a, sent_b, recv_b
+):
+    me = lax.axis_index("sp")
+    peers = [lax.rem(me + r, sp) for r in range(1, sp)]
+    greet([on_mesh(sp=peer) for peer in peers])
+    pl.semaphore_wait(pltpu.get_barrier_semaphore(), sp - 1)
+    out = []
+    for part in range(2):
+        for r, peer in enumerate(peers):
+            out.append(
+                send(
+                    maps_ref.at[part, peer],
+                    got.at[part, me],
+                    sent_a.at[part, r],
+                    recv_a.at[part, me],
+                    on_mesh(sp=peer),
+                )
+            )
+            out[-1].start()
+    got[:, me] = maps_ref[:, me]
+
+    def arrive(part):
+        for peer in peers:
+            send(
+                got.at[part, peer], got.at[part, peer], sent_a.at[part, 0], recv_a.at[part, peer], on_mesh(sp=peer)
+            ).wait_recv()
+
+    def at(step, slot):
+        reverse = lax.rem(me * per + slot, 2)
+        return step + reverse * (sp - 1 - 2 * step)
+
+    arrive(0)
+    states = [jnp.zeros((HEAD_DIM, HEAD_DIM), f32) for slot in range(per)]
+    for step in range(sp):
+        for slot in range(per):
+            states[slot] = apply_maps(got[0, at(step, slot), slot], states[slot])
+    arrive(1)
+    for step in range(sp):
+        for slot in range(per):
+            place = at(step, slot)
+            starts[place, slot] = states[slot].astype(bf16)
+
+            @pl.when(place != me)
+            def _():
+                send(
+                    starts.at[place, slot],
+                    back.at[me, slot],
+                    sent_b.at[place, slot],
+                    recv_b.at[me, slot],
+                    on_mesh(sp=place),
+                ).start()
+
+            if step < sp - 1:
+                states[slot] = apply_maps(got[1, place, slot], states[slot])
+    back[me] = starts[me]
+    for peer in peers:
+        for slot in range(per):
+            send(
+                back.at[peer, slot], back.at[peer, slot], sent_b.at[peer, slot], recv_b.at[peer, slot], on_mesh(sp=peer)
+            ).wait_recv()
+    for head in range(o_ref.shape[0]):
+        pair = [back[item // per, item % per] for item in (2 * head, 2 * head + 1)]
+        combined = o_ref[head] + jnp.dot(
+            e_ref[head], jnp.concatenate(pair, axis=0), preferred_element_type=f32
+        )
+        scale = lax.rsqrt(jnp.mean(combined * combined, axis=1, keepdims=True) + epsilon)
+        out_ref[:, head * HEAD_DIM : (head + 1) * HEAD_DIM] = (combined * scale * gain_ref[...]).astype(bf16)
+    for copy in out:
+        copy.wait_send()
+    for peer in peers:
+        for slot in range(per):
+            send(
+                starts.at[peer, slot],
+                back.at[me, slot],
+                sent_b.at[peer, slot],
+                recv_b.at[me, slot],
+                on_mesh(sp=peer),
+            ).wait_send()
+
+
+def exchange(maps, local, early, gain):
     heads, tokens, _ = local.shape
+    items = maps.shape[1]
+    sp = lax.axis_size("sp")
+    per = -(-items // sp)
+    padded = jnp.pad(maps, ((0, 0), (0, per * sp - items), (0, 0), (0, 0)))
+    padded = padded.reshape((2, sp, per) + maps.shape[2:])
+    vmem = pl.BlockSpec(memory_space=pltpu.VMEM)
     return pl.pallas_call(
-        finish_kernel,
-        grid=(heads,),
-        in_specs=[
-            pl.BlockSpec((1, tokens, HEAD_DIM), lambda h: (h, 0, 0)),
-            pl.BlockSpec((1, tokens, 2 * HEAD_DIM), lambda h: (h, 0, 0)),
-            pl.BlockSpec((2, HEAD_DIM, HEAD_DIM), lambda h: (h, 0, 0)),
-            pl.BlockSpec((1, HEAD_DIM), lambda h: (0, 0)),
-        ],
-        out_specs=pl.BlockSpec((tokens, HEAD_DIM), lambda h: (0, h)),
+        functools.partial(exchange_kernel, sp, per),
+        in_specs=[vmem] * 4,
+        out_specs=vmem,
         out_shape=jax.ShapeDtypeStruct((tokens, heads * HEAD_DIM), bf16),
-        name="finish",
-    )(local, early, starts, gain)
-
-
-def start_states(maps):
-    items = maps.shape[0]
-    peers = lax.axis_size("sp")
-    per = -(-items // peers)
-    padded = jnp.pad(maps, ((0, per * peers - items), (0, 0), (0, 0), (0, 0)))
-    padded = padded.reshape((peers, per) + maps.shape[1:])
-    mine = lax.all_to_all(padded, "sp", 0, 0)
-    starts = pl.pallas_call(
-        functools.partial(chain_kernel, peers, per),
-        out_shape=jax.ShapeDtypeStruct((peers, per, HEAD_DIM, HEAD_DIM), bf16),
-        name="chain",
-    )(mine)
-    back = lax.all_to_all(starts, "sp", 0, 0)
-    return back.reshape(peers * per, HEAD_DIM, HEAD_DIM)[:items]
+        scratch_shapes=[
+            pltpu.VMEM(padded.shape, bf16),
+            pltpu.VMEM((sp, per, HEAD_DIM, HEAD_DIM), bf16),
+            pltpu.VMEM((sp, per, HEAD_DIM, HEAD_DIM), bf16),
+            pltpu.SemaphoreType.DMA((2, sp)),
+            pltpu.SemaphoreType.DMA((2, sp)),
+            pltpu.SemaphoreType.DMA((sp, per)),
+            pltpu.SemaphoreType.DMA((sp, per)),
+        ],
+        compiler_params=pltpu.CompilerParams(
+            collective_id=1, has_side_effects=True, vmem_limit_bytes=48 * 1024 * 1024
+        ),
+        name="exchange",
+    )(padded, local, early, gain)
 
 
 def rms_rows(row_data, row_gain):
@@ -276,17 +410,7 @@
     tokens, ctx_tokens = latent.shape[0], context.shape[0]
     stacked = jnp.stack([condition, context_condition]).astype(f32)
     silu_rows = jax.nn.silu(stacked).astype(bf16)
-    partial_rows = jnp.concatenate(
-        [
-            jnp.dot(silu_rows, shift_weight, preferred_element_type=f32),
-            jnp.dot(silu_rows, scale_weight, preferred_element_type=f32),
-            jnp.dot(silu_rows[:1], gate_weight, preferred_element_type=f32),
-        ],
-        axis=0,
-    )
-    summed = jnp.sum(lax.all_gather(partial_rows, "sp"), axis=0)
-    gate_row = summed[4]
-    rows = lax.all_gather(summed[:4], "tp", axis=1, tiled=True)
+    rows, gate_row = modulation(silu_rows, shift_weight, scale_weight, gate_weight)
 
     def modulate(row_data, row_index):
         normed = rms_rows(row_data, norm_gain)
@@ -318,8 +442,7 @@
     col = jnp.transpose(gates, (3, 0, 1, 2)).reshape(heads_here, tokens + ctx_tokens, 4)
     row = jnp.transpose(gates, (3, 1, 2, 0)).reshape(heads_here, 4, tokens + ctx_tokens)
     local, early, maps = prepare(queries, keys, values, col, row, tokens, ctx_tokens)
-    starts = start_states(maps.reshape((heads_here * 2, 2) + maps.shape[3:]))
-    head_out = finish(local, early, starts, head_gain[None, :])
+    head_out = exchange(maps, local, early, head_gain[None, :])
     branch = jnp.dot(
         lax.all_gather(head_out, "tp", axis=1, tiled=True), out_weight, preferred_element_type=f32
     )

time: 188 us -> 157 us (0.84)
  blocking collectives: 82.4 us -> 0 us
  Pallas kernels: 30.8 us -> 80.3 us
  local copies, waits for them, and re-layouts: 6.69 us -> 11 us
  waiting for transfers between devices: 21.7 us -> 19.3 us
    pallas_call x2, Pallas kernels: 8.26 us -> 57.7 us  [the longest x1 40.5 us: exchange(): pl.pallas_call(functools.partial(exchange_kernel, sp, per), in_specs=[vme...]
    all_to_all x2 -> x0, blocking collectives: 44.6 us -> none  [the longest x1 31.9 us: start_states(): mine = lax.all_to_all(padded, 'sp', 0, 0)]
    all_gather x2 -> x0, blocking collectives: 37.8 us -> none  [the longest x1 32.6 us: body(): summed = jnp.sum(lax.all_gather(partial_rows, 'sp'), axis=0)]
    unnamed x24 -> x28, local copies, waits for them, and re-layouts: 1.99 us -> 5.69 us
    all_gather x1, waiting for transfers between devices: 21.7 us -> 19.3 us  [body(): lax.all_gather(head_out, 'tp', axis=1, tiled=True)]
where the time goes in v2:
time: 157 us
  Pallas kernels  80.3 us (51%)
  matrix products  22.3 us (14%)
  waiting for transfers between devices  19.3 us (12%)
  between operations  13.6 us (9%)
  local copies, waits for them, and re-layouts  11 us (7%)
  other arithmetic  10.2 us (6%)
    pallas_call x1, Pallas kernels, exchange(): pl.pallas_call(functools.partial(exchange_kernel, sp, per), in_specs=[vme...  40.5 us
    pallas_call x1, Pallas kernels, prepare(): pl.pallas_call(functools.partial(prep_kernel, tokens, ctx_tokens), grid=(...  22.6 us
    all_gather x1, waiting for transfers between devices, body(): lax.all_gather(head_out, 'tp', axis=1, tiled=True)  19.3 us
    pallas_call x1, Pallas kernels, modulation(): pl.pallas_call(functools.partial(modulation_kernel, sp, tp), in_specs=[vm...  17.3 us
    dot_general x4, matrix products, project(): return jnp.dot(matrix, weight, preferred_element_type=f32).astype(bf16)  15.2 us
    dot_general x1, matrix products, body(): jnp.dot(lax.all_gather(head_out, 'tp', axis=1, tiled=True), out_weight, p...  6.4 us
    unnamed x28, local copies, waits for them, and re-layouts  5.69 us
    reduce_sum x2, other arithmetic, rms_rows(): jnp.mean(values * values, axis=-1, keepdims=True) + epsilon  4.39 us
  transfers between devices with their start and end apart: 1, of which 1 were waited for; matrix products, arithmetic and copies ran while one was open for 0% of the time, Pallas kernels for 0%

profile of v2, /device:TPU:0, one launch (start us, length us, event | category | flops | bytes accessed | tf_op | source)
XLA Modules:
  0.0 156.8 jit_solution(18068877417577200913)
XLA Ops:
  6.5 1.3 fusion.6
  7.9 0.7 stack.34
  8.6 0.7 stack.35
  9.2 3.1 %fusion = f32[512]{0:T(512)S(1)} fusion(bf16[512,4096]{1,0:T(8,128)(2,1)} %param.18), kind=kLoop, calls=%fused_computation.2 | loop fusion | flops 6290944 | bytes 4196352 | tf_op jit(solution)/shard_map/reduce_sum | solution.py:370
  12.4 0.6 pad.4.silu_ref
  13.0 17.3 %modulation.1 = (f32[4,4096]{1,0:T(4,128)}, f32[1,1024]{1,0:T(1,128)}) custom-call(bf16[8,512]{1,0:T(8,128)(2,1)} %pad.4.silu_ref, bf16[512,1024]{1,0:T(8,128)(2,1)} %shift_ref.1, bf16[512,1024]{1,0:T(8,128)(2,1)} %scale_ref.1, bf16[512,1024]{1,0:T(8,128)(2,1)} %gate_ref.1), custom_call_target="tpu_custom_call" | custom-call | tf_op jit(solution)/shard_map/modulation/pallas_call | solution.py:240
  30.2 1.1 slice_add_fusion.1
  31.4 0.1 fusion.41
  31.5 1.0 constant_dynamic-slice_fusion.3
  32.6 0.3 fusion.10
  32.9 4.1 %fusion.4 = bf16[512,4096]{1,0:T(8,128)(2,1)S(1)} fusion(bf16[512,4096]{1,0:T(8,128)(2,1)} %param.18, f32[4096]{0:T(1024)S(1)} %bitcast.90, f32[4096]{0:T(1024)S(1)} %bitcast.89, f32[4096]{0:T(1024)S(1)} %copy-done.7, f32[512]{0:T(512)S(1)} %add_rsqrt_fusion), kind=kLoop, calls=%fused_computation.6 | loop fusion | flops 12582912 | bytes 8439808 | tf_op jit(solution)/shard_map/convert_element_type | solution.py:417
  36.9 2.0 %copy-done.4 = bf16[512,4096]{1,0:T(8,128)(2,1)} copy-done((bf16[512,4096]{1,0:T(8,128)(2,1)}, bf16[512,4096]{1,0:T(8,128)(2,1)S(1)}, u32[]{:S(2)}) %copy-start.4) | copy-done | bytes 4194328
  38.9 1.3 fusion.5
  40.3 0.1 constant_dynamic-slice_fusion
  40.4 0.1 fusion.26
  40.5 0.1 convolution_bitcast_fusion.2
  40.6 0.2 convolution_bitcast_fusion.3
  40.8 0.2 convolution_bitcast_fusion
  41.0 0.2 convolution_bitcast_fusion.1
  41.3 0.1 fusion.32
  41.4 0.6 reshape.97.row_ref
  42.1 7.0 %convolution_convert_fusion.1.k_ref = bf16[576,512]{1,0:T(8,128)(2,1)} fusion(bf16[4096,512]{1,0:T(8,128)(2,1)} %param.27, bf16[64,4096]{1,0:T(8,128)(2,1)S(1)} %fusion.10, bf16[512,4096]{1,0:T(8,128)(2,1)} %copy-done.4), kind=kOutput, calls=%fused_computation.10 | convolution fusion | flops 2425651200 | bytes 9502720 | tf_op jit(solution)/shard_map/dot_general | solution.py:375
  49.1 3.4 %convolution_convert_fusion.v_ref = bf16[576,512]{1,0:T(8,128)(2,1)} fusion(bf16[4096,512]{1,0:T(8,128)(2,1)S(1)} %copy-done.11, bf16[64,4096]{1,0:T(8,128)(2,1)S(1)} %fusion.10, bf16[512,4096]{1,0:T(8,128)(2,1)S(1)} %copy-done.5), kind=kOutput, calls=%fused_computation.9 | convolution fusion | flops 2425651200 | bytes 9502720 | tf_op jit(solution)/shard_map/dot_general | solution.py:375
  52.6 3.4 %convolution_convert_fusion.2.q_ref = bf16[576,512]{1,0:T(8,128)(2,1)} fusion(bf16[4096,512]{1,0:T(8,128)(2,1)S(1)} %copy-done.12, bf16[64,4096]{1,0:T(8,128)(2,1)S(1)} %fusion.10, bf16[512,4096]{1,0:T(8,128)(2,1)S(1)} %copy-done.5), kind=kOutput, calls=%fused_computation.11 | convolution fusion | flops 2425651200 | bytes 9502720 | tf_op jit(solution)/shard_map/dot_general | solution.py:375
  56.0 1.5 copy.25.col_ref
  57.5 22.6 %prepare.1 = (f32[4,512,128]{2,1,0:T(8,128)}, bf16[4,512,256]{2,1,0:T(8,128)(2,1)}, bf16[2,8,128,256]{3,2,1,0:T(8,128)(2,1)}) custom-call(bf16[576,512]{1,0:T(8,128)(2,1)} %convolution_convert_fusion.2.q_ref, bf16[576,512]{1,0:T(8,128)(2,1)} %convolution_convert_fusion.1.k_ref, bf16[576,512]{1,0:T(8,128)(2,1)} %convolution_convert_fusion.v_ref, ...), custom_call_target="tpu_custom_call" | custom-call | tf_op jit(solution)/shard_map/prepare/pallas_call | solution.py:140
  80.1 1.2 copy-done
  81.3 1.2 copy-done.1
  82.5 1.2 copy-done.2
  83.7 40.5 %exchange.1 = bf16[512,512]{1,0:T(8,128)(2,1)} custom-call(bf16[2,8,1,128,256]{4,3,2,1,0:T(8,128)(2,1)S(1)} %bitcast.86, f32[4,512,128]{2,1,0:T(8,128)S(1)} %copy-done, bf16[4,512,256]{2,1,0:T(8,128)(2,1)S(1)} %copy-done.1, f32[1,128]{1,0:T(1,128)S(1)} %bitcast.87), custom_call_target="tpu_custom_call" | custom-call | tf_op jit(solution)/shard_map/exchange/pallas_call | solution.py:347
  124.2 19.3 %all-gather.2.cloned.1.call-done = bf16[512,2048]{1,0:T(8,128)(2,1)} async-done(((bf16[512,512]{1,0:T(8,128)(2,1)}), bf16[512,2048]{1,0:T(8,128)(2,1)}) %all-gather.2.cloned.1.call-update) | async-done | bytes 2097168 | tf_op jit(solution)/shard_map/all_gather | solution.py:447
  143.6 6.4 %add_convert_fusion = bf16[512,1024]{1,0:T(8,128)(2,1)} fusion(bf16[512,2048]{1,0:T(8,128)(2,1)} %all-gather.2.cloned.1.call-done, bf16[2048,1024]{1,0:T(8,128)(2,1)} %param.35, f32[1024]{0:T(1024)S(1)} %bitcast.93, bf16[512,4096]{1,0:T(8,128)(2,1)} %param.18, s32[]{:T(128)S(6)} %select_n.26), kind=kOutput, calls=%fused_computation.8 | convolution fusion | flops 2149580800 | bytes 8392708 | tf_op jit(solution)/shard_map/dot_general | solution.py:446
  (39 shorter events, 0.2 us)
Async XLA Ops:
  6.5 24.8 %copy-start.8 = (f32[2,16]{1,0:T(2,128)S(1)}, f32[2,16]{1,0:T(2,128)}, u32[]{:S(2)}) copy-start(f32[2,16]{1,0:T(2,128)} %param.33) | copy-start | bytes 388
  6.5 137.0 %all-gather.2.cloned.1.call-start = ((), (), s32[]{:S(2)}) async-start(), calls=%async_computation | async-start | bytes 2621440 | tf_op jit(solution)/shard_map/all_gather | solution.py:447
  6.5 26.0 %copy-start.6 = (bf16[64,4096]{1,0:T(8,128)(2,1)S(1)}, bf16[64,4096]{1,0:T(8,128)(2,1)}, u32[]{:S(2)}) copy-start(bf16[64,4096]{1,0:T(8,128)(2,1)} %param.19) | copy-start | bytes 1572868
  6.5 26.0 %copy-start.7 = (f32[4096]{0:T(1024)S(1)}, f32[4096]{0:T(1024)}, u32[]{:S(2)}) copy-start(f32[4096]{0:T(1024)} %param.25) | copy-start | bytes 49156
  36.9 2.0 %copy-start.4 = (bf16[512,4096]{1,0:T(8,128)(2,1)}, bf16[512,4096]{1,0:T(8,128)(2,1)S(1)}, u32[]{:S(2)}) copy-start(bf16[512,4096]{1,0:T(8,128)(2,1)S(1)} %fusion.4) | copy-start | bytes 12582916
  38.9 1.4 copy-start.9
  38.9 1.4 copy-start.10
  42.1 7.0 %copy-start.5 = (bf16[512,4096]{1,0:T(8,128)(2,1)S(1)}, bf16[512,4096]{1,0:T(8,128)(2,1)}, u32[]{:S(2)}) copy-start(bf16[512,4096]{1,0:T(8,128)(2,1)} %copy-done.4) | copy-start | bytes 12582916
  42.1 7.0 %copy-start.11 = (bf16[4096,512]{1,0:T(8,128)(2,1)S(1)}, bf16[4096,512]{1,0:T(8,128)(2,1)}, u32[]{:S(2)}) copy-start(bf16[4096,512]{1,0:T(8,128)(2,1)} %param.28) | copy-start | bytes 12582916
  49.1 3.4 %copy-start.12 = (bf16[4096,512]{1,0:T(8,128)(2,1)S(1)}, bf16[4096,512]{1,0:T(8,128)(2,1)}, u32[]{:S(2)}) copy-start(bf16[4096,512]{1,0:T(8,128)(2,1)} %param.26) | copy-start | bytes 12582916
  56.0 24.1 %copy-start.3 = (f32[128]{0:T(128)S(1)}, f32[128]{0:T(128)}, u32[]{:S(2)}) copy-start(f32[128]{0:T(128)} %param.34) | copy-start | bytes 1540
  56.0 87.6 %copy-start.13 = (f32[1,1024]{1,0:T(1,128)S(1)}, f32[1,1024]{1,0:T(1,128)}, u32[]{:S(2)}) copy-start(f32[1,1024]{1,0:T(1,128)} %get-tuple-element.10) | copy-start | bytes 12292
  80.1 1.2 copy-start
  81.3 1.2 copy-start.1
  82.5 1.2 copy-start.2
Sparse Core Ops, SparseCore 0:
  124.4 19.1 all-gather.1

commit v3 on v2

--- a/solution.py
+++ b/solution.py
@@ -365,6 +365,110 @@
     )(padded, local, early, gain)
 
 
+def output_kernel(
+    tp, pieces, head_ref, gate_ref, latent_ref, weight_ref, out_ref,
+    got, weight, residual, acc, local_sems, sent_y, recv_y, sent_c, recv_c, sent_r, recv_r,
+):
+    me, col = lax.axis_index("sp"), lax.axis_index("tp")
+    core = lax.rem(col, 2)
+    partner = col + 1 - 2 * core
+    chips = tp // 2
+    far = [lax.rem(col + 2 * r, tp) for r in range(1, chips)]
+    far_partner = [place + 1 - 2 * core for place in far]
+    tokens, depth = head_ref.shape
+    width = out_ref.shape[1]
+    rows = tokens // pieces
+    load = pltpu.make_async_copy(weight_ref, weight, local_sems.at[0])
+    load.start()
+    take = pltpu.make_async_copy(
+        latent_ref.at[:, pl.ds(pl.multiple_of(col * width, width), width)], residual, local_sems.at[1]
+    )
+    take.start()
+    greet([on_mesh(tp=place) for place in [partner] + far])
+    pl.semaphore_wait(pltpu.get_barrier_semaphore(), chips)
+    out = []
+
+    def piece(ref, p):
+        return ref.at[pl.ds(p * rows, rows)]
+
+    for p in range(pieces):
+        for r, place in enumerate(far):
+            out.append(
+                send(piece(head_ref, p), piece(got.at[col], p), sent_y.at[r, p], recv_y.at[col, p], on_mesh(tp=place))
+            )
+            out[-1].start()
+    for p in range(pieces):
+        out.append(
+            send(piece(head_ref, p), piece(got.at[col], p), sent_c.at[p], recv_c.at[p], on_mesh(tp=partner))
+        )
+        out[-1].start()
+    load.wait()
+
+    def weights(src):
+        return weight[pl.ds(pl.multiple_of(src * depth, depth), depth), :]
+
+    def add(p, block, src, first=False):
+        part = jnp.dot(block, weights(src), preferred_element_type=f32)
+        at = pl.ds(p * rows, rows)
+        acc[at, :] = part if first else acc[at, :] + part
+
+    for p in range(pieces):
+        add(p, head_ref[pl.ds(p * rows, rows), :], col, True)
+    for p in range(pieces):
+        spot = piece(got.at[partner], p)
+        send(spot, spot, sent_c.at[p], recv_c.at[p], on_mesh(tp=partner)).wait_recv()
+        add(p, spot[...], partner)
+    take.wait()
+    for p in range(pieces):
+        for r, src in enumerate(far):
+            spot = piece(got.at[src], p)
+            send(spot, spot, sent_y.at[r, p], recv_y.at[src, p], on_mesh(tp=src)).wait_recv()
+            out.append(send(spot, spot, sent_r.at[r, p], recv_r.at[src, p], on_mesh(tp=partner)))
+            out[-1].start()
+            add(p, spot[...], src)
+        for r, src in enumerate(far_partner):
+            spot = piece(got.at[src], p)
+            send(spot, spot, sent_r.at[r, p], recv_r.at[src, p], on_mesh(tp=partner)).wait_recv()
+            add(p, spot[...], src)
+        at = pl.ds(p * rows, rows)
+        out_ref[at, :] = (residual[at, :].astype(f32) + gate_ref[...] * acc[at, :]).astype(bf16)
+    for copy in out:
+        copy.wait_send()
+
+
+def output(head_out, gate_row, latent, out_weight):
+    tp = lax.axis_size("tp")
+    tokens, depth = head_out.shape
+    width = out_weight.shape[1]
+    pieces = 4
+    vmem = pl.BlockSpec(memory_space=pltpu.VMEM)
+    anywhere = pl.BlockSpec(memory_space=pl.ANY)
+    dma = pltpu.SemaphoreType.DMA
+    return pl.pallas_call(
+        functools.partial(output_kernel, tp, pieces),
+        in_specs=[vmem, vmem, anywhere, anywhere],
+        out_specs=vmem,
+        out_shape=jax.ShapeDtypeStruct((tokens, width), bf16),
+        scratch_shapes=[
+            pltpu.VMEM((tp, tokens, depth), bf16),
+            pltpu.VMEM(out_weight.shape, bf16),
+            pltpu.VMEM((tokens, width), bf16),
+            pltpu.VMEM((tokens, width), f32),
+            dma((2,)),
+            dma((tp, pieces)),
+            dma((tp, pieces)),
+            dma((pieces,)),
+            dma((pieces,)),
+            dma((tp, pieces)),
+            dma((tp, pieces)),
+        ],
+        compiler_params=pltpu.CompilerParams(
+            collective_id=2, has_side_effects=True, vmem_limit_bytes=48 * 1024 * 1024
+        ),
+        name="output",
+    )(head_out, gate_row, latent, out_weight)
+
+
 def rms_rows(row_data, row_gain):
     values = row_data.astype(f32)
     scaled = values * lax.rsqrt(jnp.mean(values * values, axis=-1, keepdims=True) + epsilon)
@@ -405,8 +509,6 @@
 ):
     heads_here = query_weight.shape[1] // HEAD_DIM
     first_head = lax.axis_index("tp") * heads_here
-    own_cols = gate_weight.shape[1]
-    col_start = lax.axis_index("tp") * own_cols
     tokens, ctx_tokens = latent.shape[0], context.shape[0]
     stacked = jnp.stack([condition, context_condition]).astype(f32)
     silu_rows = jax.nn.silu(stacked).astype(bf16)
@@ -443,11 +545,7 @@
     row = jnp.transpose(gates, (3, 1, 2, 0)).reshape(heads_here, 4, tokens + ctx_tokens)
     local, early, maps = prepare(queries, keys, values, col, row, tokens, ctx_tokens)
     head_out = exchange(maps, local, early, head_gain[None, :])
-    branch = jnp.dot(
-        lax.all_gather(head_out, "tp", axis=1, tiled=True), out_weight, preferred_element_type=f32
-    )
-    residual = lax.dynamic_slice_in_dim(latent, col_start, own_cols, 1).astype(f32)
-    return (residual + gate_row * branch).astype(bf16)
+    return output(head_out, gate_row, latent, out_weight)
 
 
 def solution(mesh):

time: 157 us -> 137 us (0.87)
  waiting for transfers between devices: 19.3 us -> 0 us
  Pallas kernels: 80.3 us -> 95.2 us
  between operations: 13.6 us -> 0.23 us
  matrix products: 22.3 us -> 15.9 us
  local copies, waits for them, and re-layouts: 11 us -> 14.2 us
    all_gather x1 -> x0, waiting for transfers between devices: 19.3 us -> none  [body(): lax.all_gather(head_out, 'tp', axis=1, tiled=True)]
    pallas_call x0 -> x1, Pallas kernels: none -> 15.7 us  [output(): pl.pallas_call(functools.partial(output_kernel, tp, pieces), in_specs=[vm...]
    dot_general x1 -> x0, matrix products: 6.4 us -> none  [body(): jnp.dot(lax.all_gather(head_out, 'tp', axis=1, tiled=True), out_weight, p...]
    unnamed x28 -> x29, local copies, waits for them, and re-layouts: 5.69 us -> 8.84 us
  transfers between devices with their start and end apart: 1 -> 0, of which waited for: 1 -> 0; matrix products, arithmetic and copies ran while one was open for 0% -> 0% of each run, Pallas kernels for 0% -> 0%
where the time goes in v3:
time: 137 us; the launch traced here: 136 us
  Pallas kernels  95.2 us (69%)
  matrix products  15.9 us (12%)
  local copies, waits for them, and re-layouts  14.2 us (10%)
  other arithmetic  10.8 us (8%)
    pallas_call x1, Pallas kernels, exchange(): pl.pallas_call(functools.partial(exchange_kernel, sp, per), in_specs=[vme...  39.7 us
    pallas_call x1, Pallas kernels, prepare(): pl.pallas_call(functools.partial(prep_kernel, tokens, ctx_tokens), grid=(...  22.6 us
    pallas_call x1, Pallas kernels, modulation(): pl.pallas_call(functools.partial(modulation_kernel, sp, tp), in_specs=[vm...  17.2 us
    pallas_call x1, Pallas kernels, output(): pl.pallas_call(functools.partial(output_kernel, tp, pieces), in_specs=[vm...  15.7 us
    dot_general x4, matrix products, project(): return jnp.dot(matrix, weight, preferred_element_type=f32).astype(bf16)  15.2 us
    unnamed x29, local copies, waits for them, and re-layouts  8.84 us
    reduce_sum x2, other arithmetic, rms_rows(): jnp.mean(values * values, axis=-1, keepdims=True) + epsilon  4.4 us
    convert_element_type x2, other arithmetic, modulate(): return (normed * (1.0 + rows[2 + row_index]) + rows[row_index]).astype(bf16)  4.34 us

profile of v3, /device:TPU:0, one launch (start us, length us, event | category | flops | bytes accessed | tf_op | source)
XLA Modules:
  0.0 136.3 jit_solution(14543206035404452542)
XLA Ops:
  0.0 1.3 fusion.6
  1.3 0.8 fusion.41
  2.1 0.7 stack.34
  2.8 0.7 stack.35
  3.5 3.1 %fusion = f32[512]{0:T(512)S(1)} fusion(bf16[512,4096]{1,0:T(8,128)(2,1)} %latent_ref.1), kind=kLoop, calls=%fused_computation.2 | loop fusion | flops 6290944 | bytes 4196352 | tf_op jit(solution)/shard_map/reduce_sum | solution.py:474
  6.7 0.6 pad.4.silu_ref
  7.3 17.2 %modulation.1 = (f32[4,4096]{1,0:T(4,128)}, f32[1,1024]{1,0:T(1,128)}) custom-call(bf16[8,512]{1,0:T(8,128)(2,1)} %pad.4.silu_ref, bf16[512,1024]{1,0:T(8,128)(2,1)} %shift_ref.1, bf16[512,1024]{1,0:T(8,128)(2,1)} %scale_ref.1, bf16[512,1024]{1,0:T(8,128)(2,1)} %gate_ref.1), custom_call_target="tpu_custom_call" | custom-call | tf_op jit(solution)/shard_map/modulation/pallas_call | solution.py:240
  24.5 1.1 slice_add_fusion.1
  25.6 1.0 constant_dynamic-slice_fusion.3
  26.7 0.3 fusion.10
  27.0 4.1 %fusion.4 = bf16[512,4096]{1,0:T(8,128)(2,1)S(1)} fusion(bf16[512,4096]{1,0:T(8,128)(2,1)} %latent_ref.1, f32[4096]{0:T(1024)S(1)} %bitcast.87, f32[4096]{0:T(1024)S(1)} %bitcast.86, f32[4096]{0:T(1024)S(1)} %copy-done.9, f32[512]{0:T(512)S(1)} %add_rsqrt_fusion), kind=kLoop, calls=%fused_computation.6 | loop fusion | flops 12582912 | bytes 8439808 | tf_op jit(solution)/shard_map/convert_element_type | solution.py:519
  31.1 2.0 %copy-done.6 = bf16[512,4096]{1,0:T(8,128)(2,1)} copy-done((bf16[512,4096]{1,0:T(8,128)(2,1)}, bf16[512,4096]{1,0:T(8,128)(2,1)S(1)}, u32[]{:S(2)}) %copy-start.6) | copy-done | bytes 4194328
  33.1 1.3 fusion.5
  34.4 0.1 fusion.26
  34.5 0.1 fusion.32
  34.6 0.1 convolution_bitcast_fusion.2
  34.8 0.2 convolution_bitcast_fusion.3
  35.0 0.2 convolution_bitcast_fusion
  35.2 0.2 convolution_bitcast_fusion.1
  35.5 0.7 reshape.97.row_ref
  36.1 7.0 %convolution_convert_fusion.1.k_ref = bf16[576,512]{1,0:T(8,128)(2,1)} fusion(bf16[4096,512]{1,0:T(8,128)(2,1)} %param.27, bf16[64,4096]{1,0:T(8,128)(2,1)S(1)} %fusion.10, bf16[512,4096]{1,0:T(8,128)(2,1)} %copy-done.6), kind=kOutput, calls=%fused_computation.9 | convolution fusion | flops 2425651200 | bytes 9502720 | tf_op jit(solution)/shard_map/dot_general | solution.py:479
  43.2 3.4 %convolution_convert_fusion.v_ref = bf16[576,512]{1,0:T(8,128)(2,1)} fusion(bf16[4096,512]{1,0:T(8,128)(2,1)S(1)} %copy-done.12, bf16[64,4096]{1,0:T(8,128)(2,1)S(1)} %fusion.10, bf16[512,4096]{1,0:T(8,128)(2,1)S(1)} %copy-done.7), kind=kOutput, calls=%fused_computation.8 | convolution fusion | flops 2425651200 | bytes 9502720 | tf_op jit(solution)/shard_map/dot_general | solution.py:479
  46.6 3.4 %convolution_convert_fusion.2.q_ref = bf16[576,512]{1,0:T(8,128)(2,1)} fusion(bf16[4096,512]{1,0:T(8,128)(2,1)S(1)} %copy-done.13, bf16[64,4096]{1,0:T(8,128)(2,1)S(1)} %fusion.10, bf16[512,4096]{1,0:T(8,128)(2,1)S(1)} %copy-done.7), kind=kOutput, calls=%fused_computation.10 | convolution fusion | flops 2425651200 | bytes 9502720 | tf_op jit(solution)/shard_map/dot_general | solution.py:479
  50.0 1.5 %copy.25.col_ref = f32[4,576,4]{2,1,0:T(8,128)} copy(f32[4,576,4]{1,0,2:T(4,128)S(1)} %bitcast.85) | data formatting | bytes 73728 | tf_op jit(solution)/shard_map/reshape | solution.py:544
  51.5 22.6 %prepare.1 = (f32[4,512,128]{2,1,0:T(8,128)}, bf16[4,512,256]{2,1,0:T(8,128)(2,1)}, bf16[2,8,128,256]{3,2,1,0:T(8,128)(2,1)}) custom-call(bf16[576,512]{1,0:T(8,128)(2,1)} %convolution_convert_fusion.2.q_ref, bf16[576,512]{1,0:T(8,128)(2,1)} %convolution_convert_fusion.1.k_ref, bf16[576,512]{1,0:T(8,128)(2,1)} %convolution_convert_fusion.v_ref, ...), custom_call_target="tpu_custom_call" | custom-call | tf_op jit(solution)/shard_map/prepare/pallas_call | solution.py:140
  74.1 1.2 copy-done.1
  75.3 1.2 copy-done.2
  76.5 1.2 copy-done.3
  77.8 39.7 %exchange.1.head_ref = bf16[512,512]{1,0:T(8,128)(2,1)S(1)} custom-call(bf16[2,8,1,128,256]{4,3,2,1,0:T(8,128)(2,1)S(1)} %bitcast.83, f32[4,512,128]{2,1,0:T(8,128)S(1)} %copy-done.1, bf16[4,512,256]{2,1,0:T(8,128)(2,1)S(1)} %copy-done.2, f32[1,128]{1,0:T(1,128)S(1)} %bitcast.84), custom_call_target="tpu_custom_call" | custom-call | tf_op jit(solution)/shard_map/exchange/pallas_call | solution.py:347
  117.5 2.2 %copy-done = bf16[512,4096]{1,0:T(8,128)(2,1)S(1)} copy-done((bf16[512,4096]{1,0:T(8,128)(2,1)S(1)}, bf16[512,4096]{1,0:T(8,128)(2,1)}, u32[]{:S(2)}) %copy-start) | copy-done | bytes 4194328
  119.7 15.7 %output.1 = bf16[512,1024]{1,0:T(8,128)(2,1)S(1)} custom-call(bf16[512,512]{1,0:T(8,128)(2,1)S(1)} %exchange.1.head_ref, f32[1,1024]{1,0:T(1,128)S(1)} %copy-done.4, bf16[512,4096]{1,0:T(8,128)(2,1)S(1)} %copy-done, bf16[2048,1024]{1,0:T(8,128)(2,1)} %weight_ref.1), custom_call_target="tpu_custom_call" | custom-call | tf_op jit(solution)/shard_map/output/pallas_call | solution.py:447
  135.4 1.0 copy.27
  (37 shorter events, 0.3 us)
Async XLA Ops:
  0.0 6.6 %copy-start.10 = (f32[2,16]{1,0:T(2,128)S(1)}, f32[2,16]{1,0:T(2,128)}, u32[]{:S(2)}) copy-start(f32[2,16]{1,0:T(2,128)} %param.32) | copy-start | bytes 388
  0.0 6.6 %copy-start.11 = (f32[2,16]{1,0:T(2,128)S(1)}, f32[2,16]{1,0:T(2,128)}, u32[]{:S(2)}) copy-start(f32[2,16]{1,0:T(2,128)} %param.31) | copy-start | bytes 388
  0.0 26.7 %copy-start.8 = (bf16[64,4096]{1,0:T(8,128)(2,1)S(1)}, bf16[64,4096]{1,0:T(8,128)(2,1)}, u32[]{:S(2)}) copy-start(bf16[64,4096]{1,0:T(8,128)(2,1)} %param.19) | copy-start | bytes 1572868
  0.0 26.7 %copy-start.9 = (f32[4096]{0:T(1024)S(1)}, f32[4096]{0:T(1024)}, u32[]{:S(2)}) copy-start(f32[4096]{0:T(1024)} %param.25) | copy-start | bytes 49156
  31.1 2.0 %copy-start.6 = (bf16[512,4096]{1,0:T(8,128)(2,1)}, bf16[512,4096]{1,0:T(8,128)(2,1)S(1)}, u32[]{:S(2)}) copy-start(bf16[512,4096]{1,0:T(8,128)(2,1)S(1)} %fusion.4) | copy-start | bytes 12582916
  36.1 7.0 %copy-start.7 = (bf16[512,4096]{1,0:T(8,128)(2,1)S(1)}, bf16[512,4096]{1,0:T(8,128)(2,1)}, u32[]{:S(2)}) copy-start(bf16[512,4096]{1,0:T(8,128)(2,1)} %copy-done.6) | copy-start | bytes 12582916
  36.1 7.0 %copy-start.12 = (bf16[4096,512]{1,0:T(8,128)(2,1)S(1)}, bf16[4096,512]{1,0:T(8,128)(2,1)}, u32[]{:S(2)}) copy-start(bf16[4096,512]{1,0:T(8,128)(2,1)} %param.28) | copy-start | bytes 12582916
  43.1 3.4 %copy-start.13 = (bf16[4096,512]{1,0:T(8,128)(2,1)S(1)}, bf16[4096,512]{1,0:T(8,128)(2,1)}, u32[]{:S(2)}) copy-start(bf16[4096,512]{1,0:T(8,128)(2,1)} %param.26) | copy-start | bytes 12582916
  50.0 24.1 %copy-start.5 = (f32[128]{0:T(128)S(1)}, f32[128]{0:T(128)}, u32[]{:S(2)}) copy-start(f32[128]{0:T(128)} %param.34) | copy-start | bytes 1540
  50.0 67.5 %copy-start.4 = (f32[1,1024]{1,0:T(1,128)S(1)}, f32[1,1024]{1,0:T(1,128)}, u32[]{:S(2)}) copy-start(f32[1,1024]{1,0:T(1,128)} %get-tuple-element.14.gate_ref) | copy-start | bytes 12292
  74.1 1.2 copy-start.1
  75.3 1.2 copy-start.2
  76.5 1.2 copy-start.3
  117.5 2.2 %copy-start = (bf16[512,4096]{1,0:T(8,128)(2,1)S(1)}, bf16[512,4096]{1,0:T(8,128)(2,1)}, u32[]{:S(2)}) copy-start(bf16[512,4096]{1,0:T(8,128)(2,1)} %latent_ref.1) | copy-start | bytes 12582916

commit v4 on v3

--- a/solution.py
+++ b/solution.py
@@ -134,34 +134,6 @@
         o_ref[0, at : at + size, :] = pair[0]["out"] + pair[1]["out"]
 
 
-def prepare(queries, keys, values, col, row, tokens, ctx_tokens):
-    heads = col.shape[0]
-    every = tokens + ctx_tokens
-    return pl.pallas_call(
-        functools.partial(prep_kernel, tokens, ctx_tokens),
-        grid=(heads,),
-        in_specs=[
-            pl.BlockSpec((tokens, HEAD_DIM), lambda h: (0, h)),
-            pl.BlockSpec((every, HEAD_DIM), lambda h: (0, h)),
-            pl.BlockSpec((every, HEAD_DIM), lambda h: (0, h)),
-            pl.BlockSpec((1, every, col.shape[2]), lambda h: (h, 0, 0)),
-            pl.BlockSpec((1, row.shape[1], every), lambda h: (h, 0, 0)),
-        ],
-        out_specs=[
-            pl.BlockSpec((1, tokens, HEAD_DIM), lambda h: (h, 0, 0)),
-            pl.BlockSpec((1, tokens, 2 * HEAD_DIM), lambda h: (h, 0, 0)),
-            pl.BlockSpec((2, 2, HEAD_DIM, 2 * HEAD_DIM), lambda h: (0, h, 0, 0)),
-        ],
-        out_shape=[
-            jax.ShapeDtypeStruct((heads, tokens, HEAD_DIM), f32),
-            jax.ShapeDtypeStruct((heads, tokens, 2 * HEAD_DIM), bf16),
-            jax.ShapeDtypeStruct((2, 2 * heads, HEAD_DIM, 2 * HEAD_DIM), bf16),
-        ],
-        compiler_params=pltpu.CompilerParams(vmem_limit_bytes=60 * 1024 * 1024),
-        name="prepare",
-    )(queries, keys, values, col, row)
-
-
 def apply_maps(maps, state):
     high = state.astype(bf16)
     low = (state - high.astype(f32)).astype(bf16)
@@ -256,113 +228,156 @@
 
 
 def exchange_kernel(
-    sp, per, maps_ref, o_ref, e_ref, gain_ref, out_ref, got, starts, back, sent_a, recv_a, sent_b, recv_b
+    sp, per, tokens, ctx_tokens, q_ref, k_ref, v_ref, col_ref, row_ref, gain_ref, out_ref,
+    o_ref, e_ref, maps_ref, got, starts, back, sent_a, recv_a, sent_b, recv_b,
 ):
     me = lax.axis_index("sp")
+    heads = col_ref.shape[0]
+    items = 2 * heads
     peers = [lax.rem(me + r, sp) for r in range(1, sp)]
     greet([on_mesh(sp=peer) for peer in peers])
     pl.semaphore_wait(pltpu.get_barrier_semaphore(), sp - 1)
-    out = []
-    for part in range(2):
-        for r, peer in enumerate(peers):
-            out.append(
-                send(
-                    maps_ref.at[part, peer],
-                    got.at[part, me],
-                    sent_a.at[part, r],
-                    recv_a.at[part, me],
-                    on_mesh(sp=peer),
-                )
-            )
-            out[-1].start()
-    got[:, me] = maps_ref[:, me]
-
-    def arrive(part):
+
+    def ship(part, item):
+        owner, slot = item // per, lax.rem(item, per)
+        return owner, send(
+            maps_ref.at[part, item],
+            got.at[part, me, slot],
+            sent_a.at[part, item],
+            recv_a.at[part, me, slot],
+            on_mesh(sp=owner),
+        )
+
+    def one_head(k, unused):
+        head = lax.rem(me * per // 2 + heads // 2 + k + (heads - heads // 2 + 1), heads)
+        lanes = pl.ds(pl.multiple_of(head * HEAD_DIM, HEAD_DIM), HEAD_DIM)
+        prep_kernel(
+            tokens,
+            ctx_tokens,
+            q_ref.at[:, lanes],
+            k_ref.at[:, lanes],
+            v_ref.at[:, lanes],
+            col_ref.at[pl.ds(head, 1)],
+            row_ref.at[pl.ds(head, 1)],
+            o_ref.at[pl.ds(head, 1)],
+            e_ref.at[pl.ds(head, 1)],
+            maps_ref.at[:, pl.ds(2 * head, 2)],
+        )
+        for d in range(2):
+            for part in range(2):
+                owner, copy = ship(part, 2 * head + d)
+
+                @pl.when(owner != me)
+                def _():
+                    copy.start()
+
+                @pl.when(owner == me)
+                def _():
+                    got[part, me, lax.rem(2 * head + d, per)] = maps_ref[part, 2 * head + d]
+
+        return unused
+
+    lax.fori_loop(0, heads, one_head, 0)
+
+    def arrive(part, slot):
         for peer in peers:
-            send(
-                got.at[part, peer], got.at[part, peer], sent_a.at[part, 0], recv_a.at[part, peer], on_mesh(sp=peer)
-            ).wait_recv()
-
-    def at(step, slot):
-        reverse = lax.rem(me * per + slot, 2)
-        return step + reverse * (sp - 1 - 2 * step)
-
-    arrive(0)
-    states = [jnp.zeros((HEAD_DIM, HEAD_DIM), f32) for slot in range(per)]
-    for step in range(sp):
-        for slot in range(per):
-            states[slot] = apply_maps(got[0, at(step, slot), slot], states[slot])
-    arrive(1)
-    for step in range(sp):
-        for slot in range(per):
-            place = at(step, slot)
-            starts[place, slot] = states[slot].astype(bf16)
-
-            @pl.when(place != me)
-            def _():
-                send(
-                    starts.at[place, slot],
-                    back.at[me, slot],
-                    sent_b.at[place, slot],
-                    recv_b.at[me, slot],
-                    on_mesh(sp=place),
-                ).start()
-
-            if step < sp - 1:
-                states[slot] = apply_maps(got[1, place, slot], states[slot])
-    back[me] = starts[me]
-    for peer in peers:
-        for slot in range(per):
-            send(
-                back.at[peer, slot], back.at[peer, slot], sent_b.at[peer, slot], recv_b.at[peer, slot], on_mesh(sp=peer)
-            ).wait_recv()
-    for head in range(o_ref.shape[0]):
+            spot = got.at[part, peer, slot]
+            send(spot, spot, sent_a.at[part, 0], recv_a.at[part, peer, slot], on_mesh(sp=peer)).wait_recv()
+
+    def give_back(place, slot):
+        return send(
+            starts.at[place, slot],
+            back.at[me, slot],
+            sent_b.at[place, slot],
+            recv_b.at[me, slot],
+            on_mesh(sp=place),
+        )
+
+    for slot in range(per):
+
+        @pl.when(me * per + slot < items)
+        def _():
+            reverse = lax.rem(me * per + slot, 2)
+            arrive(0, slot)
+            state = jnp.zeros((HEAD_DIM, HEAD_DIM), f32)
+            for step in range(sp):
+                state = apply_maps(got[0, step + reverse * (sp - 1 - 2 * step), slot], state)
+            arrive(1, slot)
+            for step in range(sp):
+                place = step + reverse * (sp - 1 - 2 * step)
+                starts[place, slot] = state.astype(bf16)
+
+                @pl.when(place != me)
+                def _():
+                    give_back(place, slot).start()
+
+                @pl.when(place == me)
+                def _():
+                    back[me, slot] = starts[me, slot]
+
+                if step < sp - 1:
+                    state = apply_maps(got[1, place, slot], state)
+
+    for item in range(items):
+        owner, slot = item // per, item % per
+
+        @pl.when(owner != me)
+        def _():
+            spot = back.at[owner, slot]
+            send(spot, spot, sent_b.at[owner, slot], recv_b.at[owner, slot], on_mesh(sp=owner)).wait_recv()
+
+    for head in range(heads):
         pair = [back[item // per, item % per] for item in (2 * head, 2 * head + 1)]
         combined = o_ref[head] + jnp.dot(
             e_ref[head], jnp.concatenate(pair, axis=0), preferred_element_type=f32
         )
         scale = lax.rsqrt(jnp.mean(combined * combined, axis=1, keepdims=True) + epsilon)
         out_ref[:, head * HEAD_DIM : (head + 1) * HEAD_DIM] = (combined * scale * gain_ref[...]).astype(bf16)
-    for copy in out:
-        copy.wait_send()
-    for peer in peers:
-        for slot in range(per):
-            send(
-                starts.at[peer, slot],
-                back.at[me, slot],
-                sent_b.at[peer, slot],
-                recv_b.at[me, slot],
-                on_mesh(sp=peer),
-            ).wait_send()
-
-
-def exchange(maps, local, early, gain):
-    heads, tokens, _ = local.shape
-    items = maps.shape[1]
+    for item in range(items):
+        for part in range(2):
+            owner, copy = ship(part, item)
+
+            @pl.when(owner != me)
+            def _():
+                copy.wait_send()
+
+    for slot in range(per):
+
+        @pl.when(me * per + slot < items)
+        def _():
+            for peer in peers:
+                give_back(peer, slot).wait_send()
+
+
+def exchange(queries, keys, values, col, row, gain, tokens, ctx_tokens):
+    heads = col.shape[0]
+    items = 2 * heads
     sp = lax.axis_size("sp")
     per = -(-items // sp)
-    padded = jnp.pad(maps, ((0, 0), (0, per * sp - items), (0, 0), (0, 0)))
-    padded = padded.reshape((2, sp, per) + maps.shape[2:])
     vmem = pl.BlockSpec(memory_space=pltpu.VMEM)
+    dma = pltpu.SemaphoreType.DMA
     return pl.pallas_call(
-        functools.partial(exchange_kernel, sp, per),
-        in_specs=[vmem] * 4,
+        functools.partial(exchange_kernel, sp, per, tokens, ctx_tokens),
+        in_specs=[vmem] * 6,
         out_specs=vmem,
         out_shape=jax.ShapeDtypeStruct((tokens, heads * HEAD_DIM), bf16),
         scratch_shapes=[
-            pltpu.VMEM(padded.shape, bf16),
+            pltpu.VMEM((heads, tokens, HEAD_DIM), f32),
+            pltpu.VMEM((heads, tokens, 2 * HEAD_DIM), bf16),
+            pltpu.VMEM((2, items, HEAD_DIM, 2 * HEAD_DIM), bf16),
+            pltpu.VMEM((2, sp, per, HEAD_DIM, 2 * HEAD_DIM), bf16),
             pltpu.VMEM((sp, per, HEAD_DIM, HEAD_DIM), bf16),
             pltpu.VMEM((sp, per, HEAD_DIM, HEAD_DIM), bf16),
-            pltpu.SemaphoreType.DMA((2, sp)),
-            pltpu.SemaphoreType.DMA((2, sp)),
-            pltpu.SemaphoreType.DMA((sp, per)),
-            pltpu.SemaphoreType.DMA((sp, per)),
+            dma((2, items)),
+            dma((2, sp, per)),
+            dma((sp, per)),
+            dma((sp, per)),
         ],
         compiler_params=pltpu.CompilerParams(
             collective_id=1, has_side_effects=True, vmem_limit_bytes=48 * 1024 * 1024
         ),
         name="exchange",
-    )(padded, local, early, gain)
+    )(queries, keys, values, col, row, gain)
 
 
 def output_kernel(
@@ -463,7 +478,7 @@
             dma((tp, pieces)),
         ],
         compiler_params=pltpu.CompilerParams(
-            collective_id=2, has_side_effects=True, vmem_limit_bytes=48 * 1024 * 1024
+            collective_id=2, has_side_effects=True, vmem_limit_bytes=63 * 1024 * 1024
         ),
         name="output",
     )(head_out, gate_row, latent, out_weight)
@@ -543,8 +558,7 @@
     gates = jnp.stack([rate, running], axis=2)
     col = jnp.transpose(gates, (3, 0, 1, 2)).reshape(heads_here, tokens + ctx_tokens, 4)
     row = jnp.transpose(gates, (3, 1, 2, 0)).reshape(heads_here, 4, tokens + ctx_tokens)
-    local, early, maps = prepare(queries, keys, values, col, row, tokens, ctx_tokens)
-    head_out = exchange(maps, local, early, head_gain[None, :])
+    head_out = exchange(queries, keys, values, col, row, head_gain[None, :], tokens, ctx_tokens)
     return output(head_out, gate_row, latent, out_weight)
 
 

time: 137 us -> 112 us (0.82)
  Pallas kernels: 95.2 us -> 78 us
  local copies, waits for them, and re-layouts: 14.2 us -> 8.67 us
  matrix products: 15.9 us -> 13.4 us
    pallas_call x2 -> x1, Pallas kernels: 62.3 us -> 43.2 us  [exchange(): pl.pallas_call(functools.partial(exchange_kernel, sp, per, tokens, ctx_to...]
    unnamed x29 -> x21, local copies, waits for them, and re-layouts: 8.84 us -> 5.03 us
    dot_general x4, matrix products: 15.2 us -> 12.7 us  [project(): return jnp.dot(matrix, weight, preferred_element_type=f32).astype(bf16)]
    pallas_call x1, Pallas kernels: 15.7 us -> 17.5 us  [output(): pl.pallas_call(functools.partial(output_kernel, tp, pieces), in_specs=[vm...]
where the time goes in v4:
time: 112 us; the launch traced here: 111 us
  Pallas kernels  78 us (70%)
  matrix products  13.4 us (12%)
  other arithmetic  10.8 us (10%)
  local copies, waits for them, and re-layouts  8.67 us (8%)
    pallas_call x1, Pallas kernels, exchange(): pl.pallas_call(functools.partial(exchange_kernel, sp, per, tokens, ctx_to...  43.2 us
    pallas_call x1, Pallas kernels, output(): pl.pallas_call(functools.partial(output_kernel, tp, pieces), in_specs=[vm...  17.5 us
    pallas_call x1, Pallas kernels, modulation(): pl.pallas_call(functools.partial(modulation_kernel, sp, tp), in_specs=[vm...  17.2 us
    dot_general x4, matrix products, project(): return jnp.dot(matrix, weight, preferred_element_type=f32).astype(bf16)  12.7 us
    unnamed x21, local copies, waits for them, and re-layouts  5.03 us
    reduce_sum x2, other arithmetic, rms_rows(): jnp.mean(values * values, axis=-1, keepdims=True) + epsilon  4.4 us
    convert_element_type x2, other arithmetic, modulate(): return (normed * (1.0 + rows[2 + row_index]) + rows[row_index]).astype(bf16)  4.33 us

profile of v4, /device:TPU:0, one launch (start us, length us, event | category | flops | bytes accessed | tf_op | source)
XLA Modules:
  0.0 111.1 jit_solution(16881405424011341402)
XLA Ops:
  0.0 1.3 %fusion.6 = f32[64]{0:T(128)S(1)} fusion(bf16[64,4096]{1,0:T(8,128)(2,1)} %param.19), kind=kLoop, calls=%fused_computation.19 | loop fusion | flops 786368 | bytes 524544 | tf_op jit(solution)/shard_map/reduce_sum | solution.py:489
  1.3 0.8 fusion.41
  2.1 0.7 stack.34
  2.8 0.7 stack.35
  3.5 3.1 %fusion = f32[512]{0:T(512)S(1)} fusion(bf16[512,4096]{1,0:T(8,128)(2,1)} %latent_ref.1), kind=kLoop, calls=%fused_computation.2 | loop fusion | flops 6290944 | bytes 4196352 | tf_op jit(solution)/shard_map/reduce_sum | solution.py:489
  6.6 0.1 constant_dynamic-slice_fusion
  6.7 0.6 pad.4.silu_ref
  7.3 17.2 %modulation.1 = (f32[4,4096]{1,0:T(4,128)}, f32[1,1024]{1,0:T(1,128)}) custom-call(bf16[8,512]{1,0:T(8,128)(2,1)} %pad.4.silu_ref, bf16[512,1024]{1,0:T(8,128)(2,1)} %shift_ref.1, bf16[512,1024]{1,0:T(8,128)(2,1)} %scale_ref.1, bf16[512,1024]{1,0:T(8,128)(2,1)} %gate_ref.1), custom_call_target="tpu_custom_call" | custom-call | tf_op jit(solution)/shard_map/modulation/pallas_call | solution.py:212
  24.5 1.1 slice_add_fusion.1
  25.6 1.0 constant_dynamic-slice_fusion.3
  26.7 0.3 fusion.10
  27.0 4.1 %fusion.4 = bf16[512,4096]{1,0:T(8,128)(2,1)S(1)} fusion(bf16[512,4096]{1,0:T(8,128)(2,1)} %latent_ref.1, f32[4096]{0:T(1024)S(1)} %bitcast.85, f32[4096]{0:T(1024)S(1)} %bitcast.84, f32[4096]{0:T(1024)S(1)} %copy-done.5, f32[512]{0:T(512)S(1)} %add_rsqrt_fusion), kind=kLoop, calls=%fused_computation.6 | loop fusion | flops 12582912 | bytes 8439808 | tf_op jit(solution)/shard_map/convert_element_type | solution.py:534
  31.1 1.9 %copy-done.2 = bf16[512,4096]{1,0:T(8,128)(2,1)} copy-done((bf16[512,4096]{1,0:T(8,128)(2,1)}, bf16[512,4096]{1,0:T(8,128)(2,1)S(1)}, u32[]{:S(2)}) %copy-start.2) | copy-done | bytes 4194328
  33.0 1.3 %fusion.5 = f32[576,16]{0,1:T(8,128)S(1)} fusion(bf16[4096,8]{0,1:T(8,128)(2,1)S(1)} %reshape.85, bf16[4096,8]{0,1:T(8,128)(2,1)S(1)} %reshape.84, bf16[64,4096]{1,0:T(8,128)(2,1)S(1)} %fusion.10, bf16[512,4096]{1,0:T(8,128)(2,1)S(1)} %fusion.4), kind=kOutput, calls=%fused_computation.14 | convolution fusion | flops 85215232 | bytes 4886528 | tf_op jit(solution)/shard_map/dot_general | solution.py:494
  34.4 0.1 fusion.26
  34.5 0.1 fusion.32
  34.6 0.1 convolution_bitcast_fusion.2
  34.7 0.2 convolution_bitcast_fusion.3
  34.9 0.2 convolution_bitcast_fusion
  35.1 0.2 convolution_bitcast_fusion.1
  35.5 0.0 copy-start.8
  35.5 6.2 %convolution_convert_fusion.1.k_ref = bf16[576,512]{1,0:T(8,128)(2,1)S(1)} fusion(bf16[4096,512]{1,0:T(8,128)(2,1)} %param.27, bf16[64,4096]{1,0:T(8,128)(2,1)S(1)} %fusion.10, bf16[512,4096]{1,0:T(8,128)(2,1)} %copy-done.2), kind=kOutput, calls=%fused_computation.9 | convolution fusion | flops 2425651200 | bytes 9502720 | tf_op jit(solution)/shard_map/dot_general | solution.py:494
  41.7 0.0 copy-start.9
  41.7 2.6 %convolution_convert_fusion.v_ref = bf16[576,512]{1,0:T(8,128)(2,1)S(1)} fusion(bf16[4096,512]{1,0:T(8,128)(2,1)S(1)} %copy-done.8, bf16[64,4096]{1,0:T(8,128)(2,1)S(1)} %fusion.10, bf16[512,4096]{1,0:T(8,128)(2,1)S(1)} %copy-done.3), kind=kOutput, calls=%fused_computation.8 | convolution fusion | flops 2425651200 | bytes 9502720 | tf_op jit(solution)/shard_map/dot_general | solution.py:494
  44.3 0.0 copy-start.1
  44.4 2.6 %convolution_convert_fusion.2.q_ref = bf16[576,512]{1,0:T(8,128)(2,1)S(1)} fusion(bf16[4096,512]{1,0:T(8,128)(2,1)S(1)} %copy-done.9, bf16[64,4096]{1,0:T(8,128)(2,1)S(1)} %fusion.10, bf16[512,4096]{1,0:T(8,128)(2,1)S(1)} %copy-done.3), kind=kOutput, calls=%fused_computation.10 | convolution fusion | flops 2425651200 | bytes 9502720 | tf_op jit(solution)/shard_map/dot_general | solution.py:494
  46.9 0.4 copy.25.col_ref
  47.4 43.2 %exchange.1.head_ref = bf16[512,512]{1,0:T(8,128)(2,1)S(1)} custom-call(bf16[576,512]{1,0:T(8,128)(2,1)S(1)} %convolution_convert_fusion.2.q_ref, bf16[576,512]{1,0:T(8,128)(2,1)S(1)} %convolution_convert_fusion.1.k_ref, bf16[576,512]{1,0:T(8,128)(2,1)S(1)} %convolution_convert_fusion.v_ref, f32[4,576,4]{2,1,0:T(8,128)S(1)} %copy.25.col_ref, ...), custom_call_target="tpu_custom_call" | custom-call | tf_op jit(solution)/shard_map/exchange/pallas_call | solution.py:359
  90.6 0.0 copy-start
  90.6 0.8 copy-done
  91.4 17.5 %output.1 = bf16[512,1024]{1,0:T(8,128)(2,1)} custom-call(bf16[512,512]{1,0:T(8,128)(2,1)} %copy-done, f32[1,1024]{1,0:T(1,128)} %get-tuple-element.8.gate_ref, bf16[512,4096]{1,0:T(8,128)(2,1)} %latent_ref.1, bf16[2048,1024]{1,0:T(8,128)(2,1)} %weight_ref.1), custom_call_target="tpu_custom_call" | custom-call | tf_op jit(solution)/shard_map/output/pallas_call | solution.py:462
  108.9 2.3 %copy.27 = bf16[512,1024]{1,0:T(8,128)(2,1)} copy(bf16[512,1024]{1,0:T(8,128)(2,1)} %output.1) | data formatting | bytes 2097152
  (28 shorter events, 0.2 us)
Async XLA Ops:
  0.0 6.6 %copy-start.6 = (f32[2,16]{1,0:T(2,128)S(1)}, f32[2,16]{1,0:T(2,128)}, u32[]{:S(2)}) copy-start(f32[2,16]{1,0:T(2,128)} %param.32) | copy-start | bytes 388
  0.0 6.6 %copy-start.7 = (f32[2,16]{1,0:T(2,128)S(1)}, f32[2,16]{1,0:T(2,128)}, u32[]{:S(2)}) copy-start(f32[2,16]{1,0:T(2,128)} %param.31) | copy-start | bytes 388
  0.0 26.7 %copy-start.4 = (bf16[64,4096]{1,0:T(8,128)(2,1)S(1)}, bf16[64,4096]{1,0:T(8,128)(2,1)}, u32[]{:S(2)}) copy-start(bf16[64,4096]{1,0:T(8,128)(2,1)} %param.19) | copy-start | bytes 1572868
  0.0 26.7 %copy-start.5 = (f32[4096]{0:T(1024)S(1)}, f32[4096]{0:T(1024)}, u32[]{:S(2)}) copy-start(f32[4096]{0:T(1024)} %param.25) | copy-start | bytes 49156
  31.1 1.9 %copy-start.2 = (bf16[512,4096]{1,0:T(8,128)(2,1)}, bf16[512,4096]{1,0:T(8,128)(2,1)S(1)}, u32[]{:S(2)}) copy-start(bf16[512,4096]{1,0:T(8,128)(2,1)S(1)} %fusion.4) | copy-start | bytes 12582916
  35.5 6.2 %copy-start.3 = (bf16[512,4096]{1,0:T(8,128)(2,1)S(1)}, bf16[512,4096]{1,0:T(8,128)(2,1)}, u32[]{:S(2)}) copy-start(bf16[512,4096]{1,0:T(8,128)(2,1)} %copy-done.2) | copy-start | bytes 12582916
  35.5 6.2 %copy-start.8 = (bf16[4096,512]{1,0:T(8,128)(2,1)S(1)}, bf16[4096,512]{1,0:T(8,128)(2,1)}, u32[]{:S(2)}) copy-start(bf16[4096,512]{1,0:T(8,128)(2,1)} %param.28) | copy-start | bytes 12582916
  41.7 2.6 %copy-start.9 = (bf16[4096,512]{1,0:T(8,128)(2,1)S(1)}, bf16[4096,512]{1,0:T(8,128)(2,1)}, u32[]{:S(2)}) copy-start(bf16[4096,512]{1,0:T(8,128)(2,1)} %param.26) | copy-start | bytes 12582916
  44.3 3.0 %copy-start.1 = (f32[128]{0:T(128)S(1)}, f32[128]{0:T(128)}, u32[]{:S(2)}) copy-start(f32[128]{0:T(128)} %param.34) | copy-start | bytes 1540
  90.6 0.8 copy-start
